TPU v7x, 1024 devices: a 2x16x16 block of a 4x16x16 slice. The times are simulated.
1024 devices in a mesh: grp: 2 (over x), sp: 16 (over z), tp: 32 (over y, core).
Axes of the slice: x: 2, y: 16, z: 16, core: 2. Of those that a mesh axis runs over, the one named last changes fastest.
The devices are a block of a 4x16x16 slice.
Arguments:
- tokens: bfloat16 [4, 4096, 2048], P('grp', 'sp'), parts along dimension 0, may hold values from -6 to 6
- decoded_input: bfloat16 [4, 2048], P('grp'), parts along dimension 0, may hold values from -6 to 6
- query_weight: bfloat16 [2048, 4096], P(None, 'tp'), may hold values from -0.125 to 0.125
- key_weight: bfloat16 [2048, 4096], P(None, 'tp'), may hold values from -0.125 to 0.125
- value_weight: bfloat16 [2048, 4096], P(None, 'tp'), may hold values from -0.125 to 0.125
- gate_weight: bfloat16 [2048, 2, 32], replicated, may hold values from -0.125 to 0.125
- head_decay_rate: float32 [32], P('tp'), may hold values from 2.4414063e-05 to 0.08, as said below
- extra_log_decay: float32 [4, 32, 4096], P('grp', 'tp', 'sp'), parts along dimension 0, may hold values from -2.8 to 0, as said below
- read_norm_gain: float32 [128], replicated, may hold values from 0.1 to 1.9
Outputs:
- cache: bfloat16 [4, 32, 128, 128], P('grp', 'tp', 'sp'), parts along dimension 0
- read: bfloat16 [4, 4096], P('grp', 'tp'), parts along dimension 0
There are 2 independent parts, one for each index of `grp`. A program takes and returns all parts, laid end to end along the dimension named above; an argument that names none is the same for every part. Nothing has to cross between parts.
Inputs may be any that keep to these rules, and one draw needn't show every extreme that they name: `head_decay_rate`: positive. `extra_log_decay`: zero at all but a few positions.
All inputs are finite; a program needn't handle non-finite values.
Results may differ from a plain program's by a relative error of at most 0.002.
Values sent between devices are 32-bit elements; how exact they have to be, the bound alone decides.
A program may use at most 32 MiB of HBM per device.

v0:
```python
import jax
import jax.numpy as jnp
from jax import lax
from jax.sharding import PartitionSpec as P

BLOCK = 64


epsilon = 1e-06
write_offset = 5.0
highest = lax.Precision.HIGHEST


def prefix(shard, axis, combine, identity):
    size, mine = (lax.axis_size(axis), lax.axis_index(axis))
    everything = lax.all_gather(shard, axis)
    start = jnp.broadcast_to(jnp.asarray(identity, shard.dtype), shard.shape)

    def lap(k, before):
        at = size - 1 - k
        reached = at > mine
        new = combine(before, everything[at])
        return jnp.where(reached, new, before)

    return lax.fori_loop(0, size, lap, start)


def cut_along(shard, dim, size):
    before, after = (shard.shape[:dim], shard.shape[dim + 1 :])
    return jnp.moveaxis(shard.reshape(*before, size, -1, *after), dim, 0)


def summed_on_arrival(shard, axis, dim):
    blocks = cut_along(shard, dim, lax.axis_size(axis))
    arrived = lax.all_to_all(blocks, axis, split_axis=0, concat_axis=0, tiled=True)
    return arrived.sum(axis=0)


def sent_to_all(shard, axis):
    copies = jnp.broadcast_to(shard, (lax.axis_size(axis), *shard.shape))
    return lax.all_to_all(copies, axis, split_axis=0, concat_axis=0, tiled=True)


def taken_together(shard, axis):
    everything = sent_to_all(shard, axis)
    return jnp.sum(everything, axis=0)


def unit_rows(vectors):
    return vectors * lax.rsqrt(jnp.sum(vectors * vectors, axis=-1, keepdims=True) + epsilon)


def project(flat, key_weight, value_weight, gate_cols, head_decay_rate, head_total, head_dim):
    keys = jax.nn.silu(jnp.dot(flat, key_weight, preferred_element_type=jnp.float32))
    keys = unit_rows(keys.reshape(flat.shape[0], head_total, head_dim))
    values = jax.nn.silu(jnp.dot(flat, value_weight, preferred_element_type=jnp.float32))
    values = values.reshape(flat.shape[0], head_total, head_dim)
    gates = jnp.dot(flat, gate_cols, preferred_element_type=jnp.float32)
    beta = jax.nn.sigmoid(gates[:, :head_total] - write_offset)
    decay_factor = -head_decay_rate * jax.nn.softplus(gates[:, head_total:])
    return (keys, values, beta, decay_factor)


def block_parts(keys, values, beta, decay_factor):
    size = keys.shape[-2]
    head_dim = values.shape[-1]
    running = jnp.cumsum(decay_factor, axis=-1)
    index = jnp.arange(size)
    strict = index[:, None] > index[None, :]
    spread = running[..., :, None] - running[..., None, :]
    below = jnp.where(strict, jnp.exp(jnp.where(strict, spread, 0.0)), 0.0)
    inner = jnp.einsum("...id,...jd->...ij", keys, keys, precision=highest)
    lower = jnp.eye(size, dtype=jnp.float32) + beta[..., :, None] * inner * below
    right = jnp.concatenate(
        [values * beta[..., None], keys * (beta * jnp.exp(running))[..., None]], axis=-1
    )
    solved = jax.scipy.linalg.solve_triangular(lower, right, lower=True, unit_diagonal=True)
    total = jnp.exp(running[..., -1])
    carried = keys * jnp.exp(running[..., -1:] - running)[..., None]
    return (solved[..., :head_dim], solved[..., head_dim:], total, carried)


def product(left, right):
    return jnp.einsum("shij,shjk->shik", left, right, precision=highest)


def finish(
    state_rows,
    key_rows,
    key_read,
    query_read,
    query,
    new_key,
    new_value,
    new_beta,
    keep,
    read_norm_gain,
):
    intersection = jnp.sum(query * new_key, axis=-1)
    cache = (
        keep[..., None, None] * state_rows
        - (keep * new_beta)[..., None, None] * key_rows[..., :, None] * key_read[..., None, :]
        + new_beta[..., None, None] * key_rows[..., :, None] * new_value[..., None, :]
    )
    mixed = (
        keep[..., None] * query_read
        - (keep * new_beta * intersection)[..., None] * key_read
        + (new_beta * intersection)[..., None] * new_value
    )
    normed = (
        mixed
        * lax.rsqrt(jnp.mean(mixed * mixed, axis=-1, keepdims=True) + epsilon)
        * read_norm_gain
    )
    sequence_total = normed.shape[0]
    return (cache.astype(jnp.bfloat16), normed.reshape(sequence_total, -1).astype(jnp.bfloat16))


def per_device(
    tokens,
    decoded_input,
    query_weight,
    key_weight,
    value_weight,
    gate_weight,
    head_decay_rate,
    extra_log_decay,
    read_norm_gain,
):
    sequence_total, batch_rows, width = tokens.shape
    local_heads = head_decay_rate.shape[0]
    head_dim = key_weight.shape[1] // local_heads
    first_head = lax.axis_index("tp") * local_heads
    gate_cols = lax.dynamic_slice_in_dim(gate_weight, first_head, local_heads, 2).reshape(
        width, 2 * local_heads
    )
    flat = tokens.reshape(sequence_total * batch_rows, width)
    keys, values, beta, decay_factor = project(
        flat, key_weight, value_weight, gate_cols, head_decay_rate, local_heads, head_dim
    )
    count = batch_rows // BLOCK
    keys_b = keys.reshape(sequence_total, count, BLOCK, local_heads, head_dim).transpose(
        0, 3, 1, 2, 4
    )
    values_b = values.reshape(sequence_total, count, BLOCK, local_heads, head_dim).transpose(
        0, 3, 1, 2, 4
    )
    beta_b = beta.reshape(sequence_total, count, BLOCK, local_heads).transpose(0, 3, 1, 2)
    decay_every_token = (
        decay_factor.reshape(sequence_total, batch_rows, local_heads).transpose(0, 2, 1)
        + extra_log_decay
    )
    decay_b = decay_every_token.reshape(sequence_total, local_heads, count, BLOCK)
    solved_u, solved_w, total, carried = block_parts(keys_b, values_b, beta_b, decay_b)
    square = jnp.eye(head_dim, dtype=jnp.float32)
    change = total[..., None, None] * square - jnp.einsum(
        "shncd,shnce->shnde", carried, solved_w, precision=highest
    )
    push = jnp.einsum("shncd,shncv->shndv", carried, solved_u, precision=highest)

    def compose(carry, block):
        return ((product(block[0], carry[0]), product(block[0], carry[1]) + block[1]), None)

    identity = jnp.broadcast_to(square, (sequence_total, local_heads, head_dim, head_dim))
    empty = jnp.zeros((sequence_total, local_heads, head_dim, head_dim), jnp.float32)
    (trans_a, trans_b), _ = lax.scan(
        compose, (identity, empty), (jnp.moveaxis(change, 2, 0), jnp.moveaxis(push, 2, 0))
    )
    query = jax.nn.silu(
        jnp.dot(decoded_input, query_weight, preferred_element_type=jnp.float32)
    ).reshape(sequence_total, local_heads, head_dim)
    new_key, new_value, new_beta, new_decay = project(
        decoded_input, key_weight, value_weight, gate_cols, head_decay_rate, local_heads, head_dim
    )
    keep = jnp.exp(new_decay)
    row_count = head_dim // lax.axis_size("sp")
    row_start = lax.axis_index("sp") * row_count
    key_rows = lax.dynamic_slice_in_dim(new_key, row_start, row_count, 2)

    def multiply(earlier, later):
        return product(earlier, later)

    after = prefix(trans_a, "sp", multiply, identity)
    shares = product(after, trans_b)
    state_rows = summed_on_arrival(shares, "sp", 2)
    query_rows = lax.dynamic_slice_in_dim(query, row_start, row_count, 2)
    partial_key = jnp.einsum("shd,shdv->shv", key_rows, state_rows, precision=highest)
    partial_query = jnp.einsum("shd,shdv->shv", query_rows, state_rows, precision=highest)
    key_read, query_read = (taken_together(partial_key, "sp"), taken_together(partial_query, "sp"))
    return finish(
        state_rows,
        key_rows,
        key_read,
        query_read,
        query,
        new_key,
        new_value,
        new_beta,
        keep,
        read_norm_gain,
    )


def solution(mesh):
    in_specs = (
        P("grp", "sp", None),
        P("grp", None),
        P(None, "tp"),
        P(None, "tp"),
        P(None, "tp"),
        P(),
        P("tp"),
        P("grp", "tp", "sp"),
        P(),
    )
    out_specs = (P("grp", "tp", "sp", None), P("grp", "tp"))
    return jax.shard_map(
        per_device, mesh=mesh, in_specs=in_specs, out_specs=out_specs, check_vma=False
    )
```

profile of v0, /device:TPU:6, one launch (start us, length us, event | category | flops | bytes accessed | tf_op | source)
XLA Modules:
  0.0 300.5 jit_solution(3449348283317943820)
XLA Ops:
  8.1 0.9 constant_dynamic-slice_fusion.2
  10.7 1.8 divide_multiply_fusion
  14.0 39.3 %custom-call.4 = f32[2,4,1,64,64]{3,4,2,1,0:T(8,128)S(1)} custom-call(f32[2,4,1,64,64]{4,3,2,1,0:T(8,128)S(1)} %fusion.19), custom_call_target="InvertDiagBlocksLowerTriangular" | custom-call | tf_op jit(solution)/shard_map/jit(_solve_triangular)/vmap(vmap())/triangular_solve | solution.py:77
  54.2 1.1 convolution_bitcast_fusion.2
  55.3 1.1 fusion.14
  56.5 2.4 while.27
  59.7 1.3 multiply_reduce_fusion.3
  61.2 1.4 multiply_reduce_fusion.2
  62.6 151.7 %all-gather.3.cloned.1.call-done = f32[32,1,128,128]{3,2,1,0:T(8,128)} async-done(((f32[2,1,128,128]{3,2,1,0:T(8,128)}), f32[32,1,128,128]{3,2,1,0:T(8,128)}) %all-gather.3.cloned.1.call-update) | async-done | bytes 2097168 | tf_op jit(solution)/shard_map/all_gather | solution.py:16
  214.3 21.6 %while.28 = (s32[]{:T(128)}, f32[2,1,128,128]{2,3,0,1:T(8,128)S(1)}, s32[]{:T(128)}, f32[16,2,1,128,128]{4,3,1,0,2:T(8,128)}, s32[]{:T(128)}, /*index=5*/s32[]{:T(128)}, s32[]{:T(128)}, s32[]{:T(128)}) while((s32[]{:T(128)}, f32[2,1,128,128]{2,3,0,1:T(8,128)S(1)}, s32[]{:T(128)}, f32[16,2,1,128,128]{4,3,1,0,2:T(8,128)}, s32[]{:T(128)}, ...), condition=%wide.region_5.6_spmd, body=%wide.region_4.5_spmd.sunk | while | flops 50364424 | bytes 786585 | solution.py:25
  214.4 1.3 fusion.82
  215.8 1.3 fusion.82
  217.1 1.3 fusion.82
  218.5 1.3 fusion.82
  219.8 1.3 fusion.82
  221.2 1.3 fusion.82
  222.5 1.3 fusion.82
  223.9 1.3 fusion.82
  225.2 1.3 fusion.82
  226.6 1.3 fusion.82
  227.9 1.3 fusion.82
  229.3 1.3 fusion.82
  230.6 1.3 fusion.82
  232.0 1.3 fusion.82
  233.3 1.3 fusion.82
  234.7 1.3 fusion.82
  237.0 8.1 %all-to-all-start = ((f32[16,2,1,8,128]{4,3,1,2,0:T(8,128)}), f32[16,2,1,8,128]{4,3,1,2,0:T(8,128)S(1)}, u32[]{:S(2)}, u32[]{:S(2)}) async-start(f32[16,2,1,8,128]{4,3,1,2,0:T(8,128)} %bitcast.139), calls=%async_computation | async-start | bytes 262144 | tf_op jit(solution)/shard_map/all_to_all | solution.py:35
  245.2 12.7 %all-to-all-done = f32[16,2,1,8,128]{4,3,1,2,0:T(8,128)S(1)} async-done(((f32[16,2,1,8,128]{4,3,1,2,0:T(8,128)}), f32[16,2,1,8,128]{4,3,1,2,0:T(8,128)S(1)}, u32[]{:S(2)}, u32[]{:S(2)}) %all-to-all-start) | async-done | bytes 131104 | tf_op jit(solution)/shard_map/all_to_all | solution.py:35
  258.8 4.2 %all-to-all-start.1 = ((f32[16,2,1,128]{3,2,1,0:T(1,128)}), f32[16,2,1,128]{3,2,1,0:T(1,128)S(1)}, u32[]{:S(2)}, u32[]{:S(2)}) async-start(f32[16,2,1,128]{3,2,1,0:T(1,128)} %broadcast_in_dim.31), calls=%async_computation.1 | async-start | bytes 32768 | tf_op jit(solution)/shard_map/all_to_all | solution.py:41
  263.2 12.2 %all-to-all-done.1 = f32[16,2,1,128]{3,2,1,0:T(1,128)S(1)} async-done(((f32[16,2,1,128]{3,2,1,0:T(1,128)}), f32[16,2,1,128]{3,2,1,0:T(1,128)S(1)}, u32[]{:S(2)}, u32[]{:S(2)}) %all-to-all-start.1) | async-done | bytes 16416 | tf_op jit(solution)/shard_map/all_to_all | solution.py:41
  276.0 3.9 %all-to-all-start.2 = ((f32[16,2,1,128]{3,2,1,0:T(1,128)}), f32[16,2,1,128]{3,2,1,0:T(1,128)S(1)}, u32[]{:S(2)}, u32[]{:S(2)}) async-start(f32[16,2,1,128]{3,2,1,0:T(1,128)} %broadcast_in_dim.32), calls=%async_computation.2 | async-start | bytes 32768 | tf_op jit(solution)/shard_map/all_to_all | solution.py:41
  280.0 12.0 %all-to-all-done.2 = f32[16,2,1,128]{3,2,1,0:T(1,128)S(1)} async-done(((f32[16,2,1,128]{3,2,1,0:T(1,128)}), f32[16,2,1,128]{3,2,1,0:T(1,128)S(1)}, u32[]{:S(2)}, u32[]{:S(2)}) %all-to-all-start.2) | async-done | bytes 16416 | tf_op jit(solution)/shard_map/all_to_all | solution.py:41
  (91 shorter events, 12.0 us)
Async XLA Ops:
  7.2 1.8 copy-start
  7.2 2.5 copy-start.4
  7.2 207.1 %all-gather.3.cloned.1.call-start = ((), (), s32[]{:S(2)}) async-start(), calls=%async_computation.3 | async-start | bytes 2228224 | tf_op jit(solution)/shard_map/all_gather | solution.py:16
  9.6 2.8 copy-start.2
  56.5 3.2 %copy-start.3 = (bf16[2,2048]{1,0:T(2,128)(2,1)S(1)}, bf16[2,2048]{1,0:T(2,128)(2,1)}, u32[]{:S(2)}) copy-start(bf16[2,2048]{1,0:T(2,128)(2,1)} %param.14) | copy-start | bytes 24580
  58.9 0.7 copy-start.1
  214.3 77.7 %copy-start.6 = (bf16[2048,128]{1,0:T(8,128)(2,1)S(1)}, bf16[2048,128]{1,0:T(8,128)(2,1)}, u32[]{:S(2)}) copy-start(bf16[2048,128]{1,0:T(8,128)(2,1)} %param.17) | copy-start | bytes 1572868
  214.3 78.7 %copy-start.5 = (f32[128]{0:T(128)S(1)}, f32[128]{0:T(128)}, u32[]{:S(2)}) copy-start(f32[128]{0:T(128)} %param.21) | copy-start | bytes 1540
  237.0 21.0 %all-to-all-start = ((f32[16,2,1,8,128]{4,3,1,2,0:T(8,128)}), f32[16,2,1,8,128]{4,3,1,2,0:T(8,128)S(1)}, u32[]{:S(2)}, u32[]{:S(2)}) async-start(f32[16,2,1,8,128]{4,3,1,2,0:T(8,128)} %bitcast.139), calls=%async_computation | async-start | bytes 262144 | tf_op jit(solution)/shard_map/all_to_all | solution.py:35
  258.8 16.6 %all-to-all-start.1 = ((f32[16,2,1,128]{3,2,1,0:T(1,128)}), f32[16,2,1,128]{3,2,1,0:T(1,128)S(1)}, u32[]{:S(2)}, u32[]{:S(2)}) async-start(f32[16,2,1,128]{3,2,1,0:T(1,128)} %broadcast_in_dim.31), calls=%async_computation.1 | async-start | bytes 32768 | tf_op jit(solution)/shard_map/all_to_all | solution.py:41
  276.0 16.0 %all-to-all-start.2 = ((f32[16,2,1,128]{3,2,1,0:T(1,128)}), f32[16,2,1,128]{3,2,1,0:T(1,128)S(1)}, u32[]{:S(2)}, u32[]{:S(2)}) async-start(f32[16,2,1,128]{3,2,1,0:T(1,128)} %broadcast_in_dim.32), calls=%async_computation.2 | async-start | bytes 32768 | tf_op jit(solution)/shard_map/all_to_all | solution.py:41
Sparse Core Ops, SparseCore 0:
  59.7 154.5 all-gather.2
where the time goes:
time: 301 us; the launch traced here: 300 us
  waiting for transfers between devices  189 us (63%)
  other arithmetic  42 us (14%)
  matrix products  33.4 us (11%)
  starting transfers between devices  16.3 us (5%)
  between operations  15.1 us (5%)
  local copies, waits for them, and re-layouts  4.2 us (1%)
    all_gather x1, waiting for transfers between devices, prefix(): everything = lax.all_gather(shard, axis)  152 us
    another operation x2, other arithmetic, block_parts(): jax.scipy.linalg.solve_triangular(lower, right, lower=True, unit_diagonal...  39.3 us
    all_to_all x2, waiting for transfers between devices, sent_to_all(): return lax.all_to_all(copies, axis, split_axis=0, concat_axis=0, tiled=True)  24.2 us
    dot_general x25, matrix products, product(): return jnp.einsum('shij,shjk->shik', left, right, precision=highest)  23.3 us
    all_to_all x1, waiting for transfers between devices, summed_on_arrival(): lax.all_to_all(blocks, axis, split_axis=0, concat_axis=0, tiled=True)  12.7 us
    all_to_all x2, starting transfers between devices, sent_to_all(): return lax.all_to_all(copies, axis, split_axis=0, concat_axis=0, tiled=True)  8.18 us
    all_to_all x1, starting transfers between devices, summed_on_arrival(): lax.all_to_all(blocks, axis, split_axis=0, concat_axis=0, tiled=True)  8.06 us
  transfers between devices with their start and end apart: 4, of which 4 were waited for; matrix products, arithmetic and copies ran while one was open for 1% of the time, Pallas kernels for 0%

commit v1 on v0

v1 whole, which is shorter than its diff:
```python
import functools

import jax
import jax.numpy as jnp
from jax import lax
from jax.experimental import pallas as pl
from jax.experimental.pallas import tpu as pltpu
from jax.sharding import PartitionSpec as P

MESH = pl.DeviceIdType.MESH
F32 = jnp.float32
BF16 = jnp.bfloat16
epsilon = 1e-06
write_offset = 5.0
QUAD = 4


def split(x):
    hi = x.astype(BF16)
    lo = (x - hi.astype(F32)).astype(BF16)
    return hi, lo


def dot(a, b):
    return jnp.dot(a, b, preferred_element_type=F32)


def dot_nt(a, b):
    return lax.dot_general(a, b, (((1,), (1,)), ((), ())), preferred_element_type=F32)


def product(a, b, one=dot):
    ah, al = split(a)
    bh, bl = split(b)
    return one(ah, bh) + (one(ah, bl) + one(al, bh))


def silu(x):
    return x * jax.nn.sigmoid(x)


def softplus(x):
    return jnp.maximum(x, 0.0) + jnp.log1p(jnp.exp(-jnp.abs(x)))


def unit_rows(x):
    return x * lax.rsqrt(jnp.sum(x * x, axis=-1, keepdims=True) + epsilon)


def iota(shape, dim):
    return lax.broadcasted_iota(jnp.int32, shape, dim)


def kernel(
    seqs,
    rows,
    count,
    tok_hbm,
    dec_ref,
    wq_hbm,
    wk_hbm,
    wv_hbm,
    gate_ref,
    rate_ref,
    extra_ref,
    gain_ref,
    cache_ref,
    read_ref,
    x_ref,
    wkv_ref,
    wq_ref,
    k_ref,
    v_ref,
    n_ref,
    t_ref,
    ab_ref,
    rx1_ref,
    c1_ref,
    rx2_ref,
    c2_ref,
    rxa_ref,
    rxb_ref,
    ft_ref,
    tx_ref,
    tiles_ref,
    new_ref,
    load_sem,
    send1,
    recv1,
    send2,
    recv2,
    send_a,
    recv_a,
    send_b,
    recv_b,
    send_s,
    recv_s,
):
    me = lax.axis_index("sp")
    head = k_ref.shape[-1]
    mine = lax.rem(me, 2)
    quad = me // QUAD
    rank = lax.rem(me, QUAD)
    low = rank < 2
    is_even = mine == 0

    loads = [
        pltpu.make_async_copy(wk_hbm, wkv_ref.at[:, pl.ds(0, head)], load_sem.at[0]),
        pltpu.make_async_copy(wv_hbm, wkv_ref.at[:, pl.ds(head, head)], load_sem.at[1]),
    ]
    for s in range(seqs):
        loads.append(pltpu.make_async_copy(tok_hbm.at[s], x_ref.at[s], load_sem.at[2 + s]))
    loads.append(pltpu.make_async_copy(wq_hbm, wq_ref, load_sem.at[2 + seqs]))
    for load in loads:
        load.start()

    barrier = pltpu.get_barrier_semaphore()
    for k in range(1, count):
        pl.semaphore_signal(
            barrier, inc=1, device_id={"sp": lax.rem(me + k, count)}, device_id_type=MESH
        )

    loads[0].wait()
    loads[1].wait()

    gate_rows = []
    for s in range(seqs):
        loads[2 + s].wait()
        kv = silu(dot(x_ref[s], wkv_ref[...]))
        k_ref[s] = unit_rows(kv[:, :head])
        v_ref[s] = kv[:, head:]
        gate_rows.append(jnp.transpose(dot(x_ref[s], gate_ref[...])))
    rate = rate_ref[0]
    betas = [jax.nn.sigmoid(g[0:1] - write_offset) for g in gate_rows]
    decays = [-rate * softplus(g[1:2]) + extra_ref[s] for s, g in enumerate(gate_rows)]
    stacked = jnp.concatenate(decays, axis=0)
    hi, rest = split(stacked)
    rest32 = stacked - hi.astype(F32)
    lo = (rest32 - rest.astype(F32)).astype(BF16)
    row_i = iota((rows, rows), 0)
    col_i = iota((rows, rows), 1)
    upto = jnp.where(row_i <= col_i, 1.0, 0.0).astype(BF16)
    running = dot(hi, upto) + (dot(rest, upto) + dot(lo, upto))
    last = running[:, rows - 1 : rows]
    packed = jnp.concatenate(
        betas
        + [running, jnp.exp(running), jnp.exp(last - running)],
        axis=0,
    )
    columns = jnp.transpose(packed)

    def column(kind, s):
        at = kind * seqs + s
        return columns[:, at : at + 1]

    for s in range(seqs):
        keys = k_ref[s]
        inner = product(keys, keys, dot_nt)
        spread = column(1, s) - running[s : s + 1]
        strict = row_i > col_i
        below = jnp.where(strict, jnp.exp(jnp.where(strict, spread, 0.0)), 0.0)
        n_mat = column(0, s) * inner * below
        n_ref[s] = n_mat
        pair = jnp.logical_and(lax.shift_right_logical(row_i, 1) == lax.shift_right_logical(col_i, 1), strict)
        t_ref[s] = jnp.where(row_i == col_i, 1.0, 0.0) - jnp.where(pair, n_mat, 0.0)

    levels = rows.bit_length() - 1

    def level(at, carry):
        ri = lax.shift_right_logical(row_i, at)
        ci = lax.shift_right_logical(col_i, at)
        mask = jnp.logical_and(ri == ci + 1, lax.bitwise_and(ci, 1) == 0)
        for s in range(seqs):
            t_mat = t_ref[s]
            inner = product(jnp.where(mask, n_ref[s], 0.0), t_mat)
            t_ref[s] = t_mat - product(t_mat, inner)
        return carry

    lax.fori_loop(1, levels, level, 0)

    head_eye = jnp.where(iota((head, head), 0) == iota((head, head), 1), 1.0, 0.0)
    for s in range(seqs):
        keys = k_ref[s]
        right = jnp.concatenate(
            [keys * (column(0, s) * column(2, s)), v_ref[s] * column(0, s)], axis=1
        )
        solved = product(t_ref[s], right)
        both = product(jnp.transpose(solved), keys * column(3, s))
        ab_ref[s, :head] = jnp.exp(last[s : s + 1]) * head_eye - both[:head]
        ab_ref[s, head:] = both[head:]

    pl.semaphore_wait(barrier, count - 1)

    def other(flip):
        return {"sp": lax.bitwise_xor(me, flip)}

    copy1 = pltpu.make_async_remote_copy(
        src_ref=ab_ref.at[1 - mine],
        dst_ref=rx1_ref,
        send_sem=send1,
        recv_sem=recv1,
        device_id=other(1),
        device_id_type=MESH,
    )
    copy1.start()

    loads[2 + seqs].wait()
    dec = dec_ref[...]
    new_kv = silu(dot(dec, wkv_ref[...]))
    new_key = unit_rows(new_kv[:, :head])
    new_value = new_kv[:, head:]
    query = silu(dot(dec, wq_ref[...]))
    new_gate = dot(dec, gate_ref[...])
    new_beta = jax.nn.sigmoid(new_gate[:, 0:1] - write_offset)
    keep = jnp.exp(-rate * softplus(new_gate[:, 1:2]))
    for s in range(seqs):
        at = slice(s, s + 1)
        new_ref[s, 0:1] = new_key[at]
        new_ref[s, 1:2] = query[at]
        new_ref[s, 2:3] = new_value[at]
        new_ref[s, 3:4] = jnp.broadcast_to(new_beta[at], (1, head))
        new_ref[s, 4:5] = jnp.broadcast_to(keep[at], (1, head))
        new_ref[s, 5:8] = jnp.zeros((3, head), F32)

    copy1.wait()
    kept = ab_ref[mine]
    got = rx1_ref[...]
    left = jnp.where(is_even, kept, got)
    right = jnp.where(is_even, got, kept)
    both = product(left, right[:head])
    c1_ref[:head] = both[:head]
    c1_ref[head:] = both[head:] + right[head:]

    copy2 = pltpu.make_async_remote_copy(
        src_ref=c1_ref.at[pl.ds(pl.multiple_of(jnp.where(low, head, 0), head), head)],
        dst_ref=rx2_ref,
        send_sem=send2,
        recv_sem=recv2,
        device_id=other(2),
        device_id_type=MESH,
    )
    copy2.start()
    copy2.wait()
    own = c1_ref[:head]
    got = rx2_ref[...]
    both = product(jnp.where(low, own, got), jnp.where(low, got, own))
    c2_ref[...] = both + jnp.where(low, 0.0, c1_ref[head:])

    quads = count // QUAD
    share = head // quads

    def copy_a(k):
        return pltpu.make_async_remote_copy(
            src_ref=c2_ref,
            dst_ref=rxa_ref.at[quad],
            send_sem=send_a.at[k],
            recv_sem=recv_a.at[quad],
            device_id={"sp": lax.rem(quad + k, quads) * QUAD + rank},
            device_id_type=MESH,
        )

    def copy_b(k):
        to = lax.rem(quad + k, quads)
        return pltpu.make_async_remote_copy(
            src_ref=c2_ref.at[pl.ds(pl.multiple_of(to * share, share), share)],
            dst_ref=rxb_ref.at[quad],
            send_sem=send_b.at[k],
            recv_sem=recv_b.at[quad],
            device_id={"sp": to * QUAD + rank - 2},
            device_id_type=MESH,
        )

    far_first = sorted(range(quads), key=lambda k: -min(k, quads - k))

    @pl.when(jnp.logical_and(low, quad > 0))
    def _():
        for k in far_first:
            if k:
                copy_a(k).start()

    @pl.when(jnp.logical_not(low))
    def _():
        for k in far_first:
            copy_b(k).start()

    def arrival(ref, slot, sem, shape_ref):
        return pltpu.make_async_remote_copy(
            src_ref=shape_ref,
            dst_ref=ref.at[slot],
            send_sem=send1,
            recv_sem=sem.at[slot],
            device_id=other(1),
            device_id_type=MESH,
        )

    slot_mine = mine * quads + quad

    def copy_s(k):
        to = lax.rem(me + k, count)
        return pltpu.make_async_remote_copy(
            src_ref=tx_ref.at[pl.ds(pl.multiple_of(to * 8, 8), 8)],
            dst_ref=tiles_ref.at[slot_mine],
            send_sem=send_s.at[k],
            recv_sem=recv_s.at[slot_mine],
            device_id={"sp": to},
            device_id_type=MESH,
        )

    lane = iota((1, head), 1)

    @pl.when(low)
    def _():
        rxa_ref[quad] = c2_ref[...]
        arrival(rxb_ref, 0, recv_b, c2_ref.at[pl.ds(0, share)]).wait_recv()
        state = rxb_ref[0]
        for g in range(1, quads):

            @pl.when(quad != g)
            def _():
                arrival(rxa_ref, g, recv_a, c2_ref).wait_recv()

            arrival(rxb_ref, g, recv_b, c2_ref.at[pl.ds(0, share)]).wait_recv()
            state = product(state, rxa_ref[g]) + rxb_ref[g]
        ft_ref[...] = jnp.zeros((head, head), F32)
        ft_ref[pl.ds(pl.multiple_of(quad * share, share), share)] = state
        final = jnp.transpose(ft_ref[...])
        new = new_ref[mine]
        reads = product(new, final)
        key_read, query_read = reads[0:1], reads[1:2]
        beta, hold = new[3:4], new[4:5]
        value = jnp.where(lane // share == quad, new[2:3], 0.0)
        inter = jnp.sum(new[0:1] * new[1:2], axis=-1, keepdims=True)
        key_col = jnp.transpose(new)[:, 0:1]
        cache = hold * final - (hold * beta) * key_col * key_read + beta * key_col * value
        mixed = hold * query_read - (hold * beta * inter) * key_read + (beta * inter) * value
        moved = pltpu.roll(jnp.broadcast_to(mixed, (8, head)), share, 1)[0:1]
        first = lax.bitwise_and(iota((head, head), 0), 7) == 0
        tx_ref[...] = cache + jnp.where(first, moved, 0.0)
        tiles_ref[slot_mine] = tx_ref[pl.ds(pl.multiple_of(me * 8, 8), 8)]
        for k in sorted(range(1, count), key=lambda k: -min(k, count - k)):
            copy_s(k).start()

    for s in range(seqs):
        cache = jnp.zeros((8, head), F32)
        mixed = jnp.zeros((8, head), F32)
        for g in range(quads):

            @pl.when(me != g * QUAD + s)
            def _():
                arrival(tiles_ref, s * quads + g, recv_s, tx_ref.at[pl.ds(0, 8)]).wait_recv()

            tile = tiles_ref[s * quads + g]
            cache = cache + jnp.where(lane // share == g, tile, 0.0)
            mixed = mixed + jnp.where(lane // share == (g + 1) % quads, tile, 0.0)
        cache_ref[s, 0] = cache.astype(BF16)
        row = pltpu.roll(mixed, head - share, 1)[0:1]
        scale = lax.rsqrt(jnp.sum(row * row, axis=-1, keepdims=True) / head + epsilon)
        read_ref[s : s + 1] = (row * scale * gain_ref[...]).astype(BF16)

    @pl.when(jnp.logical_and(low, quad > 0))
    def _():
        for k in range(1, quads):
            copy_a(k).wait_send()

    @pl.when(jnp.logical_not(low))
    def _():
        for k in range(quads):
            copy_b(k).wait_send()

    @pl.when(low)
    def _():
        for k in range(1, count):
            copy_s(k).wait_send()


def per_device(
    tokens,
    decoded_input,
    query_weight,
    key_weight,
    value_weight,
    gate_weight,
    head_decay_rate,
    extra_log_decay,
    read_norm_gain,
):
    seqs, rows, width = tokens.shape
    head = key_weight.shape[1]
    count = lax.axis_size("sp")
    quads = count // QUAD
    gates = lax.dynamic_slice_in_dim(gate_weight, lax.axis_index("tp"), 1, 2)[:, :, 0]
    vmem = pl.BlockSpec(memory_space=pltpu.VMEM)
    hbm = pl.BlockSpec(memory_space=pl.ANY)
    dma = pltpu.SemaphoreType.DMA
    return pl.pallas_call(
        functools.partial(kernel, seqs, rows, count),
        out_shape=(
            jax.ShapeDtypeStruct((seqs, 1, head // count, head), BF16),
            jax.ShapeDtypeStruct((seqs, head), BF16),
        ),
        in_specs=[
            hbm,
            vmem,
            hbm,
            hbm,
            hbm,
            vmem,
            pl.BlockSpec(memory_space=pltpu.SMEM),
            vmem,
            vmem,
        ],
        out_specs=(vmem, vmem),
        scratch_shapes=[
            pltpu.VMEM((seqs, rows, width), BF16),
            pltpu.VMEM((width, 2 * head), BF16),
            pltpu.VMEM((width, head), BF16),
            pltpu.VMEM((seqs, rows, head), F32),
            pltpu.VMEM((seqs, rows, head), F32),
            pltpu.VMEM((seqs, rows, rows), F32),
            pltpu.VMEM((seqs, rows, rows), F32),
            pltpu.VMEM((seqs, 2 * head, head), F32),
            pltpu.VMEM((2 * head, head), F32),
            pltpu.VMEM((2 * head, head), F32),
            pltpu.VMEM((head, head), F32),
            pltpu.VMEM((head, head), F32),
            pltpu.VMEM((quads, head, head), F32),
            pltpu.VMEM((quads, head // quads, head), F32),
            pltpu.VMEM((head, head), F32),
            pltpu.VMEM((head, head), F32),
            pltpu.VMEM((seqs * quads, head // count, head), F32),
            pltpu.VMEM((seqs, 8, head), F32),
            dma((3 + seqs,)),
            dma,
            dma,
            dma,
            dma,
            dma((quads,)),
            dma((quads,)),
            dma((quads,)),
            dma((quads,)),
            dma((count,)),
            dma((seqs * quads,)),
        ],
        compiler_params=pltpu.CompilerParams(collective_id=0, has_side_effects=True),
    )(
        tokens,
        decoded_input,
        query_weight,
        key_weight,
        value_weight,
        gates,
        head_decay_rate,
        extra_log_decay,
        read_norm_gain.reshape(1, head),
    )


def solution(mesh):
    in_specs = (
        P("grp", "sp", None),
        P("grp", None),
        P(None, "tp"),
        P(None, "tp"),
        P(None, "tp"),
        P(),
        P("tp"),
        P("grp", "tp", "sp"),
        P(),
    )
    out_specs = (P("grp", "tp", "sp", None), P("grp", "tp"))
    return jax.shard_map(
        per_device, mesh=mesh, in_specs=in_specs, out_specs=out_specs, check_vma=False
    )
```

time: 301 us -> 125 us (0.42)
  waiting for transfers between devices: 189 us -> 0 us
  Pallas kernels: 0 us -> 119 us
  other arithmetic: 42 us -> 0 us
  matrix products: 33.4 us -> 0 us
  starting transfers between devices: 16.3 us -> 0 us
  between operations: 15.1 us -> 1.3 us
    all_gather x1 -> x0, waiting for transfers between devices: 152 us -> none  [prefix(): everything = lax.all_gather(shard, axis)]
    pallas_call x0 -> x1, Pallas kernels: none -> 119 us  [per_device(): pl.pallas_call(functools.partial(kernel, seqs, rows, count), out_shape=(j...]
    another operation x3 -> x0, other arithmetic: 39.8 us -> none  [the longest x2 39.3 us: block_parts(): jax.scipy.linalg.solve_triangular(lower, right, lower=True, unit_diagonal...]
    all_to_all x3 -> x0, waiting for transfers between devices: 36.9 us -> none  [the longest x2 24.2 us: sent_to_all(): return lax.all_to_all(copies, axis, split_axis=0, concat_axis=0, tiled=True)]
    dot_general x37 -> x0, matrix products: 32.7 us -> none  [the longest x25 23.3 us: product(): return jnp.einsum('shij,shjk->shik', left, right, precision=highest)]
    all_to_all x3 -> x0, starting transfers between devices: 16.2 us -> none  [the longest x2 8.18 us: sent_to_all(): return lax.all_to_all(copies, axis, split_axis=0, concat_axis=0, tiled=True)]
  transfers between devices with their start and end apart: 4 -> 0, of which waited for: 4 -> 0; matrix products, arithmetic and copies ran while one was open for 1% -> 0% of each run, Pallas kernels for 0% -> 0%
where the time goes in v1:
time: 125 us
  Pallas kernels  119 us (95%)
  local copies, waits for them, and re-layouts  4.43 us (4%)
  between operations  1.3 us (1%)
    pallas_call x1, Pallas kernels, per_device(): pl.pallas_call(functools.partial(kernel, seqs, rows, count), out_shape=(j...  119 us
    unnamed x4, local copies, waits for them, and re-layouts  3.36 us

profile of v1, /device:TPU:6, one launch (start us, length us, event | category | flops | bytes accessed | tf_op | source)
XLA Modules:
  0.0 124.9 jit_solution(18037971232850390648)
XLA Ops:
  0.6 0.0 copy-start
  0.6 0.9 copy-done
  1.6 1.0 copy.11
  3.3 119.1 %shard_map.104 = (bf16[2,1,8,128]{3,2,1,0:T(8,128)(2,1)}, bf16[2,128]{1,0:T(2,128)(2,1)}) custom-call(bf16[2,256,2048]{2,1,0:T(8,128)(2,1)} %tok_hbm.1, bf16[2,2048]{1,0:T(2,128)(2,1)} %dec_ref.1, bf16[2048,128]{1,0:T(8,128)(2,1)} %wq_hbm.1, bf16[2048,128]{1,0:T(8,128)(2,1)} %wk_hbm.1, bf16[2048,128]{1,0:T(8,128)(2,1)} %wv_hbm.1, bf16[2048,2]{1,0:T(8,128)(2,1)} %bitcast.2, ...), custom_call_target="tpu_custom_call" | custom-call | tf_op jit(solution)/shard_map/pallas_call | solution.py:395
  122.4 1.3 %copy.15 = bf16[2,1,8,128]{3,2,1,0:T(8,128)(2,1)} copy(bf16[2,1,8,128]{3,2,1,0:T(8,128)(2,1)} %get-tuple-element.4) | data formatting | bytes 8192
  123.7 1.1 copy.16
  (1 shorter events, 0.0 us)
Async XLA Ops:
  0.6 1.0 copy-start

commit v2 on v1

v2 whole, which is shorter than its diff:
```python
import functools

import jax
import jax.numpy as jnp
from jax import lax
from jax.experimental import pallas as pl
from jax.experimental.pallas import tpu as pltpu
from jax.sharding import PartitionSpec as P

MESH = pl.DeviceIdType.MESH
F32 = jnp.float32
BF16 = jnp.bfloat16
epsilon = 1e-06
write_offset = 5.0


def split(x):
    hi = x.astype(BF16)
    lo = (x - hi.astype(F32)).astype(BF16)
    return hi, lo


def dot(a, b):
    return jnp.dot(a, b, preferred_element_type=F32)


def dot_nt(a, b):
    return lax.dot_general(a, b, (((1,), (1,)), ((), ())), preferred_element_type=F32)


def product(a, b, one=dot):
    ah, al = split(a)
    bh, bl = split(b)
    return one(ah, bh) + (one(ah, bl) + one(al, bh))


def silu(x):
    return x * jax.nn.sigmoid(x)


def softplus(x):
    return jnp.maximum(x, 0.0) + jnp.log1p(jnp.exp(-jnp.abs(x)))


def unit_rows(x):
    return x * lax.rsqrt(jnp.sum(x * x, axis=-1, keepdims=True) + epsilon)


def iota(shape, dim):
    return lax.broadcasted_iota(jnp.int32, shape, dim)


def kernel(
    seqs,
    rows,
    count,
    tok_hbm,
    dec_hbm,
    wq_hbm,
    wk_hbm,
    wv_hbm,
    gate_hbm,
    rate_hbm,
    extra_hbm,
    gain_hbm,
    cache_ref,
    read_ref,
    x_ref,
    dec_ref,
    wkv_ref,
    wq_ref,
    gate_ref,
    rate_ref,
    extra_ref,
    gain_ref,
    k_ref,
    v_ref,
    n_ref,
    t_ref,
    ab_ref,
    rx_ref,
    tx_ref,
    first_ref,
    new_tx,
    new_rx,
    out_tx,
    out_rx,
    load_sem,
    send_x,
    recv_x,
    send_f,
    recv_f,
    send_n,
    recv_n,
    send_o,
    recv_o,
):
    me = lax.axis_index("sp")
    head_index = lax.axis_index("tp")
    head = k_ref.shape[-1]
    gates = gate_ref.shape[0] // 2
    last_one = count - 1
    is_first = me == 0
    is_second = me == 1
    is_last = me == last_one
    in_chain = jnp.logical_and(me > 0, me < last_one)

    def load(source, target, place):
        copy = pltpu.make_async_copy(source, target, load_sem.at[place])
        copy.start()
        return copy

    load_w = [
        load(wk_hbm, wkv_ref.at[:, pl.ds(0, head)], 0),
        load(wv_hbm, wkv_ref.at[:, pl.ds(head, head)], 1),
    ]
    load_x = [load(tok_hbm.at[0], x_ref.at[0], 2)]
    load_g = [
        load(gate_hbm, gate_ref, 3),
        load(rate_hbm, rate_ref, 4),
        load(extra_hbm, extra_ref, 5),
    ]
    for s in range(1, seqs):
        load_x.append(load(tok_hbm.at[s], x_ref.at[s], 8 + s))
    load_r = load(gain_hbm, gain_ref, 6)

    def at(index):
        return {"sp": index}

    barrier = pltpu.get_barrier_semaphore()

    def greet(index):
        pl.semaphore_signal(barrier, inc=1, device_id=at(index), device_id_type=MESH)

    @pl.when(me >= 2)
    def _():
        greet(me - 1)

    @pl.when(is_last)
    def _():
        greet(0)
        greet(1)

    @pl.when(jnp.logical_not(is_last))
    def _():
        greet(last_one)

    for copy in load_w:
        copy.wait()

    row_g = iota((gates, rows), 0)
    gate_rows = []
    for s in range(seqs):
        load_x[s].wait()
        kv = silu(dot(x_ref[s], wkv_ref[...]))
        k_ref[s] = unit_rows(kv[:, :head])
        v_ref[s] = kv[:, head:]
        if s == 0:
            for copy in load_g:
                copy.wait()
        both = dot_nt(gate_ref[...], x_ref[s])
        picked = [
            jnp.sum(jnp.where(row_g == head_index, part, 0.0), axis=0, keepdims=True)
            for part in (both[:gates], both[gates:])
        ]
        gate_rows.append(picked)
    rate = rate_ref[...]
    betas = [jax.nn.sigmoid(g[0] - write_offset) for g in gate_rows]
    decays = [-rate * softplus(g[1]) + extra_ref[s] for s, g in enumerate(gate_rows)]
    stacked = jnp.concatenate(decays, axis=0)
    hi, rest = split(stacked)
    rest32 = stacked - hi.astype(F32)
    lo = (rest32 - rest.astype(F32)).astype(BF16)
    row_i = iota((rows, rows), 0)
    col_i = iota((rows, rows), 1)
    upto = jnp.where(row_i <= col_i, 1.0, 0.0).astype(BF16)
    running = dot(hi, upto) + (dot(rest, upto) + dot(lo, upto))
    last = running[:, rows - 1 : rows]
    packed = jnp.concatenate(
        betas + [running, jnp.exp(running), jnp.exp(last - running)],
        axis=0,
    )
    columns = jnp.transpose(packed)

    def column(kind, s):
        place = kind * seqs + s
        return columns[:, place : place + 1]

    strict = row_i > col_i
    pair = jnp.logical_and(
        lax.shift_right_logical(row_i, 1) == lax.shift_right_logical(col_i, 1), strict
    )
    for s in range(seqs):
        keys = k_ref[s]
        inner = product(keys, keys, dot_nt)
        spread = column(1, s) - running[s : s + 1]
        below = jnp.where(strict, jnp.exp(jnp.where(strict, spread, 0.0)), 0.0)
        n_mat = column(0, s) * inner * below
        n_ref[s] = n_mat
        t_ref[s] = jnp.where(row_i == col_i, 1.0, 0.0) - jnp.where(pair, n_mat, 0.0)

    levels = rows.bit_length() - 1

    def level(depth, carry):
        ri = lax.shift_right_logical(row_i, depth)
        ci = lax.shift_right_logical(col_i, depth)
        mask = jnp.logical_and(ri == ci + 1, lax.bitwise_and(ci, 1) == 0)
        for s in range(seqs):
            t_mat = t_ref[s]
            inner = product(jnp.where(mask, n_ref[s], 0.0), t_mat)
            t_ref[s] = t_mat - product(t_mat, inner)
        return carry

    lax.fori_loop(1, levels, level, 0)

    head_eye = jnp.where(iota((head, head), 0) == iota((head, head), 1), 1.0, 0.0)
    for s in range(seqs):
        keys = k_ref[s]
        right = jnp.concatenate(
            [keys * (column(0, s) * column(2, s)), v_ref[s] * column(0, s)], axis=1
        )
        solved = product(t_ref[s], right)
        both = product(jnp.transpose(solved), keys * column(3, s))
        ab_ref[s, 0] = jnp.exp(last[s : s + 1]) * head_eye - both[:head]
        ab_ref[s, 1] = both[head:]

    chunks = [(s, half) for s in range(seqs) for half in range(2)]

    def chain(s, half, source):
        return pltpu.make_async_remote_copy(
            src_ref=source.at[s, half],
            dst_ref=rx_ref.at[s, half],
            send_sem=send_x.at[s, half],
            recv_sem=recv_x.at[s, half],
            device_id=at(lax.rem(me + 1, count)),
            device_id_type=MESH,
        )

    def push(s):
        return pltpu.make_async_remote_copy(
            src_ref=ab_ref.at[s, 1],
            dst_ref=first_ref.at[s],
            send_sem=send_f.at[s],
            recv_sem=recv_f.at[s],
            device_id=at(last_one),
            device_id_type=MESH,
        )

    decoded = pltpu.make_async_remote_copy(
        src_ref=new_tx,
        dst_ref=new_rx,
        send_sem=send_n,
        recv_sem=recv_n,
        device_id=at(last_one),
        device_id_type=MESH,
    )

    def rows_to(s, k):
        to = lax.rem(me + k, count)
        return pltpu.make_async_remote_copy(
            src_ref=out_tx.at[s, to],
            dst_ref=out_rx.at[s],
            send_sem=send_o.at[s, k],
            recv_sem=recv_o.at[s],
            device_id=at(to),
            device_id_type=MESH,
        )

    @pl.when(is_first)
    def _():
        pl.semaphore_wait(barrier, 1)
        for s in range(seqs):
            push(s).start()

    @pl.when(is_second)
    def _():
        pl.semaphore_wait(barrier, 2)
        for s, half in chunks:
            chain(s, half, ab_ref).start()
        copies = [
            pltpu.make_async_copy(dec_hbm, dec_ref, load_sem.at[7]),
            pltpu.make_async_copy(wq_hbm, wq_ref, load_sem.at[8]),
        ]
        for copy in copies:
            copy.start()
        for copy in copies:
            copy.wait()
        dec = dec_ref[...]
        new_kv = silu(dot(dec, wkv_ref[...]))
        new_key = unit_rows(new_kv[:, :head])
        new_value = new_kv[:, head:]
        query = silu(dot(dec, wq_ref[...]))
        both = dot_nt(gate_ref[...], dec)
        row_n = iota((gates, seqs), 0)
        picked = [
            jnp.sum(jnp.where(row_n == head_index, part, 0.0), axis=0, keepdims=True)
            for part in (both[:gates], both[gates:])
        ]
        new_beta = jax.nn.sigmoid(picked[0] - write_offset)
        keep = jnp.exp(-rate * softplus(picked[1]))
        for s in range(seqs):
            one = slice(s, s + 1)
            new_tx[s, 0:1] = new_key[one]
            new_tx[s, 1:2] = query[one]
            new_tx[s, 2:3] = new_value[one]
            new_tx[s, 3:4] = jnp.broadcast_to(new_beta[:, one], (1, head))
            new_tx[s, 4:5] = jnp.broadcast_to(keep[:, one], (1, head))
            new_tx[s, 5:8] = jnp.zeros((3, head), F32)
        decoded.start()

    @pl.when(jnp.logical_and(in_chain, me >= 2))
    def _():
        pl.semaphore_wait(barrier, 1)
        for s, half in chunks:
            chain(s, half, tx_ref).wait_recv()
            moved = product(rx_ref[s, half], ab_ref[s, 0])
            if half == 1:
                moved = moved + ab_ref[s, 1]
            tx_ref[s, half] = moved
            chain(s, half, tx_ref).start()

    @pl.when(is_last)
    def _():
        pl.semaphore_wait(barrier, count - 1)
        load_r.wait()
        decoded.wait_recv()
        for s in range(seqs):
            push(s).wait_recv()
            chain(s, 0, tx_ref).wait_recv()
            joined = product(first_ref[s], rx_ref[s, 0])
            chain(s, 1, tx_ref).wait_recv()
            joined = joined + rx_ref[s, 1]
            flipped = product(joined, ab_ref[s, 0]) + ab_ref[s, 1]
            new = new_rx[s]
            reads = product(new, flipped, dot_nt)
            final = jnp.transpose(flipped)
            key_read, query_read = reads[0:1], reads[1:2]
            value, beta, hold = new[2:3], new[3:4], new[4:5]
            inter = jnp.sum(new[0:1] * new[1:2], axis=-1, keepdims=True)
            key_col = jnp.transpose(new)[:, 0:1]
            cache = hold * final + key_col * (beta * value - (hold * beta) * key_read)
            mixed = hold * query_read - (hold * beta * inter) * key_read + (beta * inter) * value
            scale = lax.rsqrt(jnp.sum(mixed * mixed, axis=-1, keepdims=True) / head + epsilon)
            read = mixed * scale * gain_ref[...]
            each = head // count
            out_tx[s, :, :each] = cache.reshape(count, each, head)
            out_tx[s, :, each:] = jnp.broadcast_to(read.reshape(1, 1, head), (count, each, head))
            for k in range(1, count):
                rows_to(s, k).start()
            out_rx[s] = out_tx[s, last_one]

    for s in range(seqs):

        @pl.when(jnp.logical_not(is_last))
        def _():
            rows_to(s, 1).wait_recv()

        each = head // count
        cache_ref[s, 0] = out_rx[s, :each].astype(BF16)
        read_ref[s : s + 1] = out_rx[s, each : each + 1].astype(BF16)

    @pl.when(jnp.logical_not(is_last))
    def _():
        load_r.wait()

    @pl.when(is_first)
    def _():
        for s in range(seqs):
            push(s).wait_send()

    @pl.when(in_chain)
    def _():
        for s, half in chunks:
            chain(s, half, tx_ref).wait_send()

    @pl.when(is_second)
    def _():
        decoded.wait_send()

    @pl.when(is_last)
    def _():
        for s in range(seqs):
            for k in range(1, count):
                rows_to(s, k).wait_send()


def per_device(
    tokens,
    decoded_input,
    query_weight,
    key_weight,
    value_weight,
    gate_weight,
    head_decay_rate,
    extra_log_decay,
    read_norm_gain,
):
    seqs, rows, width = tokens.shape
    head = key_weight.shape[1]
    count = lax.axis_size("sp")
    each = head // count
    gates = gate_weight.transpose(1, 2, 0).reshape(-1, width)
    vmem = pl.BlockSpec(memory_space=pltpu.VMEM)
    hbm = pl.BlockSpec(memory_space=pl.ANY)
    dma = pltpu.SemaphoreType.DMA
    return pl.pallas_call(
        functools.partial(kernel, seqs, rows, count),
        out_shape=(
            jax.ShapeDtypeStruct((seqs, 1, each, head), BF16),
            jax.ShapeDtypeStruct((seqs, head), BF16),
        ),
        in_specs=[hbm] * 9,
        out_specs=(vmem, vmem),
        scratch_shapes=[
            pltpu.VMEM((seqs, rows, width), BF16),
            pltpu.VMEM((seqs, width), BF16),
            pltpu.VMEM((width, 2 * head), BF16),
            pltpu.VMEM((width, head), BF16),
            pltpu.VMEM(gates.shape, BF16),
            pltpu.VMEM((1, 1), F32),
            pltpu.VMEM((seqs, 1, rows), F32),
            pltpu.VMEM((1, head), F32),
            pltpu.VMEM((seqs, rows, head), F32),
            pltpu.VMEM((seqs, rows, head), F32),
            pltpu.VMEM((seqs, rows, rows), F32),
            pltpu.VMEM((seqs, rows, rows), F32),
            pltpu.VMEM((seqs, 2, head, head), F32),
            pltpu.VMEM((seqs, 2, head, head), F32),
            pltpu.VMEM((seqs, 2, head, head), F32),
            pltpu.VMEM((seqs, head, head), F32),
            pltpu.VMEM((seqs, 8, head), F32),
            pltpu.VMEM((seqs, 8, head), F32),
            pltpu.VMEM((seqs, count, 2 * each, head), F32),
            pltpu.VMEM((seqs, 2 * each, head), F32),
            dma((8 + seqs,)),
            dma((seqs, 2)),
            dma((seqs, 2)),
            dma((seqs,)),
            dma((seqs,)),
            dma,
            dma,
            dma((seqs, count)),
            dma((seqs,)),
        ],
        compiler_params=pltpu.CompilerParams(collective_id=0, has_side_effects=True),
    )(
        tokens,
        decoded_input,
        query_weight,
        key_weight,
        value_weight,
        gates,
        head_decay_rate.reshape(1, 1),
        extra_log_decay,
        read_norm_gain.reshape(1, head),
    )


def solution(mesh):
    in_specs = (
        P("grp", "sp", None),
        P("grp", None),
        P(None, "tp"),
        P(None, "tp"),
        P(None, "tp"),
        P(),
        P("tp"),
        P("grp", "tp", "sp"),
        P(),
    )
    out_specs = (P("grp", "tp", "sp", None), P("grp", "tp"))
    return jax.shard_map(
        per_device, mesh=mesh, in_specs=in_specs, out_specs=out_specs, check_vma=False
    )
```

time: 125 us -> 146 us (1.17)
  Pallas kernels: 119 us -> 142 us
  local copies, waits for them, and re-layouts: 4.43 us -> 2.4 us
    pallas_call x1, Pallas kernels: 119 us -> 142 us  [per_device(): pl.pallas_call(functools.partial(kernel, seqs, rows, count), out_shape=(j...]
    unnamed x4 -> x2, local copies, waits for them, and re-layouts: 3.36 us -> 2.4 us
where the time goes in v2:
time: 146 us
  Pallas kernels  142 us (97%)
  local copies, waits for them, and re-layouts  2.4 us (2%)
    pallas_call x1, Pallas kernels, per_device(): pl.pallas_call(functools.partial(kernel, seqs, rows, count), out_shape=(j...  142 us

profile of v2, /device:TPU:6, one launch (start us, length us, event | category | flops | bytes accessed | tf_op | source)
XLA Modules:
  0.0 145.6 jit_solution(975383675245931459)
XLA Ops:
  1.3 141.9 %shard_map.104 = (bf16[2,1,8,128]{3,2,1,0:T(8,128)(2,1)}, bf16[2,128]{1,0:T(2,128)(2,1)}) custom-call(bf16[2,256,2048]{2,1,0:T(8,128)(2,1)} %tok_hbm.1, bf16[2,2048]{1,0:T(2,128)(2,1)} %dec_hbm.1, bf16[2048,128]{1,0:T(8,128)(2,1)} %wq_hbm.1, bf16[2048,128]{1,0:T(8,128)(2,1)} %wk_hbm.1, bf16[2048,128]{1,0:T(8,128)(2,1)} %wv_hbm.1, bf16[64,2048]{1,0:T(8,128)(2,1)} %bitcast.6, ...), custom_call_target="tpu_custom_call" | custom-call | tf_op jit(solution)/shard_map/pallas_call | solution.py:406
  143.2 1.3 copy.14
  144.4 1.1 copy.15

commit v3 on v2

--- a/solution.py
+++ b/solution.py
@@ -12,6 +12,7 @@
 BF16 = jnp.bfloat16
 epsilon = 1e-06
 write_offset = 5.0
+BLOCK = 64
 
 
 def split(x):
@@ -28,10 +29,12 @@
     return lax.dot_general(a, b, (((1,), (1,)), ((), ())), preferred_element_type=F32)
 
 
+def passes(a, b, one=dot):
+    return one(a[0], b[0]) + (one(a[0], b[1]) + one(a[1], b[0]))
+
+
 def product(a, b, one=dot):
-    ah, al = split(a)
-    bh, bl = split(b)
-    return one(ah, bh) + (one(ah, bl) + one(al, bh))
+    return passes(split(a), split(b), one)
 
 
 def silu(x):
@@ -75,8 +78,6 @@
     gain_ref,
     k_ref,
     v_ref,
-    n_ref,
-    t_ref,
     ab_ref,
     rx_ref,
     tx_ref,
@@ -171,13 +172,20 @@
     hi, rest = split(stacked)
     rest32 = stacked - hi.astype(F32)
     lo = (rest32 - rest.astype(F32)).astype(BF16)
+    parts = (hi, rest, lo)
     row_i = iota((rows, rows), 0)
     col_i = iota((rows, rows), 1)
-    upto = jnp.where(row_i <= col_i, 1.0, 0.0).astype(BF16)
-    running = dot(hi, upto) + (dot(rest, upto) + dot(lo, upto))
-    last = running[:, rows - 1 : rows]
+    together = row_i // BLOCK == col_i // BLOCK
+    upto = jnp.where(jnp.logical_and(together, row_i <= col_i), 1.0, 0.0).astype(BF16)
+    whole = jnp.where(together, 1.0, 0.0).astype(BF16)
+    running = sum(dot(part, upto) for part in parts)
+    total = sum(dot(part, whole) for part in parts)
+    grown = jnp.exp(running)
     packed = jnp.concatenate(
-        betas + [running, jnp.exp(running), jnp.exp(last - running)],
+        betas
+        + [running]
+        + [betas[s] * grown[s : s + 1] for s in range(seqs)]
+        + [jnp.exp(total - running)],
         axis=0,
     )
     columns = jnp.transpose(packed)
@@ -186,49 +194,82 @@
         place = kind * seqs + s
         return columns[:, place : place + 1]
 
-    strict = row_i > col_i
-    pair = jnp.logical_and(
-        lax.shift_right_logical(row_i, 1) == lax.shift_right_logical(col_i, 1), strict
-    )
+    blocks = rows // BLOCK
+    row_c = iota((BLOCK, rows), 0)
+    lane_c = iota((BLOCK, rows), 1)
+    inside = lax.bitwise_and(lane_c, BLOCK - 1)
+    owner = lane_c // BLOCK
+    own_lanes = [jnp.where(owner == b, 1.0, 0.0).astype(BF16) for b in range(blocks)]
+    strict = row_c > inside
+    eye = jnp.where(row_c == inside, 1.0, 0.0)
+
+    def compact(full):
+        out = jnp.where(owner == 0, full[:BLOCK], 0.0)
+        for b in range(1, blocks):
+            out = jnp.where(owner == b, full[b * BLOCK : (b + 1) * BLOCK], out)
+        return out
+
+    def diagonal(pair):
+        return [jnp.concatenate([part * own for own in own_lanes], axis=0) for part in pair]
+
+    n_mats, solves = [], []
+    for s in range(seqs):
+        halves = split(k_ref[s])
+        inner = compact(passes(halves, halves, dot_nt))
+        spread = compact(jnp.broadcast_to(column(1, s), (rows, rows))) - running[s : s + 1]
+        below = jnp.where(strict, jnp.exp(jnp.where(strict, spread, 0.0)), 0.0)
+        n_mat = compact(jnp.broadcast_to(column(0, s), (rows, rows))) * inner * below
+        pair = row_c // 2 == inside // 2
+        n_mats.append(n_mat)
+        solves.append(eye - jnp.where(pair, n_mat, 0.0))
+    depth = 1
+    while 1 << depth < BLOCK:
+        ri = lax.shift_right_logical(row_c, depth)
+        ci = lax.shift_right_logical(inside, depth)
+        mask = jnp.logical_and(ri == ci + 1, lax.bitwise_and(ci, 1) == 0)
+        for s in range(seqs):
+            t_mat = split(solves[s])
+            inner = passes(split(jnp.where(mask, n_mats[s], 0.0)), diagonal(t_mat))
+            solves[s] = solves[s] - passes(t_mat, diagonal(split(inner)))
+        depth += 1
+
+    head_eye = jnp.where(iota((head, head), 0) == iota((head, head), 1), 1.0, 0.0)
+    row_b = iota((rows, 1), 0) // BLOCK
+    inverse = [diagonal(split(t_mat)) for t_mat in solves]
+    carried, steps = [], []
     for s in range(seqs):
         keys = k_ref[s]
-        inner = product(keys, keys, dot_nt)
-        spread = column(1, s) - running[s : s + 1]
-        below = jnp.where(strict, jnp.exp(jnp.where(strict, spread, 0.0)), 0.0)
-        n_mat = column(0, s) * inner * below
-        n_ref[s] = n_mat
-        t_ref[s] = jnp.where(row_i == col_i, 1.0, 0.0) - jnp.where(pair, n_mat, 0.0)
-
-    levels = rows.bit_length() - 1
-
-    def level(depth, carry):
-        ri = lax.shift_right_logical(row_i, depth)
-        ci = lax.shift_right_logical(col_i, depth)
-        mask = jnp.logical_and(ri == ci + 1, lax.bitwise_and(ci, 1) == 0)
-        for s in range(seqs):
-            t_mat = t_ref[s]
-            inner = product(jnp.where(mask, n_ref[s], 0.0), t_mat)
-            t_ref[s] = t_mat - product(t_mat, inner)
-        return carry
-
-    lax.fori_loop(1, levels, level, 0)
-
-    head_eye = jnp.where(iota((head, head), 0) == iota((head, head), 1), 1.0, 0.0)
+        weights = passes(inverse[s], split(keys * column(2, s)))
+        kept = keys * column(3, s)
+        spans = jnp.concatenate(
+            [jnp.where(row_b == b, kept, 0.0) for b in range(blocks)], axis=1
+        )
+        carried.append(split(spans))
+        moved = passes(split(jnp.transpose(weights)), carried[s])
+        step = []
+        for b in range(blocks):
+            decay = jnp.exp(total[s : s + 1, b * BLOCK : b * BLOCK + 1])
+            step.append(split(decay * head_eye - moved[:, b * head : (b + 1) * head]))
+        steps.append(step)
+    tails = []
     for s in range(seqs):
-        keys = k_ref[s]
-        right = jnp.concatenate(
-            [keys * (column(0, s) * column(2, s)), v_ref[s] * column(0, s)], axis=1
-        )
-        solved = product(t_ref[s], right)
-        both = product(jnp.transpose(solved), keys * column(3, s))
-        ab_ref[s, 0] = jnp.exp(last[s : s + 1]) * head_eye - both[:head]
-        ab_ref[s, 1] = both[head:]
-
-    chunks = [(s, half) for s in range(seqs) for half in range(2)]
-
-    def chain(s, half, source):
+        step = steps[s]
+        tail = split(passes(step[2], step[3]))
+        tails.append(tail)
+        ab_ref[s, 0] = passes(split(passes(step[0], step[1])), tail)
+
+    def pushes():
+        for s in range(seqs):
+            deltas = passes(inverse[s], split(v_ref[s] * column(0, s)))
+            moved = passes(split(jnp.transpose(deltas)), carried[s])
+            part = [moved[:, b * head : (b + 1) * head] for b in range(blocks)]
+            early = passes(split(part[0]), steps[s][1]) + part[1]
+            late = passes(split(part[2]), steps[s][3]) + part[3]
+            ab_ref[s, 1] = passes(split(early), tails[s]) + late
+
+    def chain(s, half):
         return pltpu.make_async_remote_copy(
-            src_ref=source.at[s, half],
+            src_ref=tx_ref.at[s, half],
             dst_ref=rx_ref.at[s, half],
             send_sem=send_x.at[s, half],
             recv_sem=recv_x.at[s, half],
@@ -266,17 +307,59 @@
             device_id_type=MESH,
         )
 
+    @pl.when(in_chain)
+    def _():
+        pl.semaphore_wait(barrier, jnp.where(is_second, 2, 1))
+
+    for s in range(seqs):
+
+        @pl.when(is_second)
+        def _():
+            tx_ref[s, 0] = ab_ref[s, 0]
+
+        @pl.when(me >= 2)
+        def _():
+            chain(s, 0).wait_recv()
+
+        @pl.when(jnp.logical_and(in_chain, me >= 2))
+        def _():
+            tx_ref[s, 0] = product(rx_ref[s, 0], ab_ref[s, 0])
+
+        @pl.when(in_chain)
+        def _():
+            if s:
+                chain(s - 1, 0).wait_send()
+            chain(s, 0).start()
+
+    pushes()
+
     @pl.when(is_first)
     def _():
         pl.semaphore_wait(barrier, 1)
         for s in range(seqs):
             push(s).start()
 
+    @pl.when(in_chain)
+    def _():
+        for s in range(seqs):
+
+            @pl.when(is_second)
+            def _():
+                tx_ref[s, 1] = ab_ref[s, 1]
+
+            @pl.when(jnp.logical_not(is_second))
+            def _():
+                chain(s, 1).wait_recv()
+                tx_ref[s, 1] = product(rx_ref[s, 1], ab_ref[s, 0]) + ab_ref[s, 1]
+
+            if s:
+                chain(s - 1, 1).wait_send()
+            else:
+                chain(seqs - 1, 0).wait_send()
+            chain(s, 1).start()
+
     @pl.when(is_second)
     def _():
-        pl.semaphore_wait(barrier, 2)
-        for s, half in chunks:
-            chain(s, half, ab_ref).start()
         copies = [
             pltpu.make_async_copy(dec_hbm, dec_ref, load_sem.at[7]),
             pltpu.make_async_copy(wq_hbm, wq_ref, load_sem.at[8]),
@@ -308,28 +391,18 @@
             new_tx[s, 5:8] = jnp.zeros((3, head), F32)
         decoded.start()
 
-    @pl.when(jnp.logical_and(in_chain, me >= 2))
-    def _():
-        pl.semaphore_wait(barrier, 1)
-        for s, half in chunks:
-            chain(s, half, tx_ref).wait_recv()
-            moved = product(rx_ref[s, half], ab_ref[s, 0])
-            if half == 1:
-                moved = moved + ab_ref[s, 1]
-            tx_ref[s, half] = moved
-            chain(s, half, tx_ref).start()
-
     @pl.when(is_last)
     def _():
         pl.semaphore_wait(barrier, count - 1)
         load_r.wait()
         decoded.wait_recv()
+        joins = []
         for s in range(seqs):
             push(s).wait_recv()
-            chain(s, 0, tx_ref).wait_recv()
-            joined = product(first_ref[s], rx_ref[s, 0])
-            chain(s, 1, tx_ref).wait_recv()
-            joined = joined + rx_ref[s, 1]
+            joins.append(product(first_ref[s], rx_ref[s, 0]))
+        for s in range(seqs):
+            chain(s, 1).wait_recv()
+            joined = joins[s] + rx_ref[s, 1]
             flipped = product(joined, ab_ref[s, 0]) + ab_ref[s, 1]
             new = new_rx[s]
             reads = product(new, flipped, dot_nt)
@@ -370,8 +443,7 @@
 
     @pl.when(in_chain)
     def _():
-        for s, half in chunks:
-            chain(s, half, tx_ref).wait_send()
+        chain(seqs - 1, 1).wait_send()
 
     @pl.when(is_second)
     def _():
@@ -422,8 +494,6 @@
             pltpu.VMEM((1, head), F32),
             pltpu.VMEM((seqs, rows, head), F32),
             pltpu.VMEM((seqs, rows, head), F32),
-            pltpu.VMEM((seqs, rows, rows), F32),
-            pltpu.VMEM((seqs, rows, rows), F32),
             pltpu.VMEM((seqs, 2, head, head), F32),
             pltpu.VMEM((seqs, 2, head, head), F32),
             pltpu.VMEM((seqs, 2, head, head), F32),

time: 146 us -> 149 us (1.021)
  Pallas kernels: 142 us -> 145 us
    pallas_call x1, Pallas kernels: 142 us -> 145 us  [per_device(): pl.pallas_call(functools.partial(kernel, seqs, rows, count), out_shape=(j...]
where the time goes in v3:
time: 149 us; the launch traced here: 148 us
  Pallas kernels  145 us (97%)
  local copies, waits for them, and re-layouts  2.4 us (2%)
    pallas_call x1, Pallas kernels, per_device(): pl.pallas_call(functools.partial(kernel, seqs, rows, count), out_shape=(j...  145 us

profile of v3, /device:TPU:6, one launch (start us, length us, event | category | flops | bytes accessed | tf_op | source)
XLA Modules:
  0.0 148.5 jit_solution(9206535124826651317)
XLA Ops:
  1.3 144.8 %shard_map.104 = (bf16[2,1,8,128]{3,2,1,0:T(8,128)(2,1)}, bf16[2,128]{1,0:T(2,128)(2,1)}) custom-call(bf16[2,256,2048]{2,1,0:T(8,128)(2,1)} %tok_hbm.1, bf16[2,2048]{1,0:T(2,128)(2,1)} %dec_hbm.1, bf16[2048,128]{1,0:T(8,128)(2,1)} %wq_hbm.1, bf16[2048,128]{1,0:T(8,128)(2,1)} %wk_hbm.1, bf16[2048,128]{1,0:T(8,128)(2,1)} %wv_hbm.1, bf16[64,2048]{1,0:T(8,128)(2,1)} %bitcast.6, ...), custom_call_target="tpu_custom_call" | custom-call | tf_op jit(solution)/shard_map/pallas_call | solution.py:478
  146.1 1.3 copy.14
  147.4 1.1 copy.15

commit v4 on v3

--- a/solution.py
+++ b/solution.py
@@ -13,6 +13,7 @@
 epsilon = 1e-06
 write_offset = 5.0
 BLOCK = 64
+GRANT = 60 * 1024 * 1024
 
 
 def split(x):
@@ -140,7 +141,6 @@
     @pl.when(is_last)
     def _():
         greet(0)
-        greet(1)
 
     @pl.when(jnp.logical_not(is_last))
     def _():
@@ -165,7 +165,7 @@
             for part in (both[:gates], both[gates:])
         ]
         gate_rows.append(picked)
-    rate = rate_ref[...]
+    rate = rate_ref[0]
     betas = [jax.nn.sigmoid(g[0] - write_offset) for g in gate_rows]
     decays = [-rate * softplus(g[1]) + extra_ref[s] for s, g in enumerate(gate_rows)]
     stacked = jnp.concatenate(decays, axis=0)
@@ -309,7 +309,7 @@
 
     @pl.when(in_chain)
     def _():
-        pl.semaphore_wait(barrier, jnp.where(is_second, 2, 1))
+        pl.semaphore_wait(barrier, 1)
 
     for s in range(seqs):
 
@@ -338,28 +338,6 @@
         pl.semaphore_wait(barrier, 1)
         for s in range(seqs):
             push(s).start()
-
-    @pl.when(in_chain)
-    def _():
-        for s in range(seqs):
-
-            @pl.when(is_second)
-            def _():
-                tx_ref[s, 1] = ab_ref[s, 1]
-
-            @pl.when(jnp.logical_not(is_second))
-            def _():
-                chain(s, 1).wait_recv()
-                tx_ref[s, 1] = product(rx_ref[s, 1], ab_ref[s, 0]) + ab_ref[s, 1]
-
-            if s:
-                chain(s - 1, 1).wait_send()
-            else:
-                chain(seqs - 1, 0).wait_send()
-            chain(s, 1).start()
-
-    @pl.when(is_second)
-    def _():
         copies = [
             pltpu.make_async_copy(dec_hbm, dec_ref, load_sem.at[7]),
             pltpu.make_async_copy(wq_hbm, wq_ref, load_sem.at[8]),
@@ -391,6 +369,25 @@
             new_tx[s, 5:8] = jnp.zeros((3, head), F32)
         decoded.start()
 
+    @pl.when(in_chain)
+    def _():
+        for s in range(seqs):
+
+            @pl.when(is_second)
+            def _():
+                tx_ref[s, 1] = ab_ref[s, 1]
+
+            @pl.when(jnp.logical_not(is_second))
+            def _():
+                chain(s, 1).wait_recv()
+                tx_ref[s, 1] = product(rx_ref[s, 1], ab_ref[s, 0]) + ab_ref[s, 1]
+
+            if s:
+                chain(s - 1, 1).wait_send()
+            else:
+                chain(seqs - 1, 0).wait_send()
+            chain(s, 1).start()
+
     @pl.when(is_last)
     def _():
         pl.semaphore_wait(barrier, count - 1)
@@ -440,14 +437,11 @@
     def _():
         for s in range(seqs):
             push(s).wait_send()
+        decoded.wait_send()
 
     @pl.when(in_chain)
     def _():
         chain(seqs - 1, 1).wait_send()
-
-    @pl.when(is_second)
-    def _():
-        decoded.wait_send()
 
     @pl.when(is_last)
     def _():
@@ -473,7 +467,7 @@
     each = head // count
     gates = gate_weight.transpose(1, 2, 0).reshape(-1, width)
     vmem = pl.BlockSpec(memory_space=pltpu.VMEM)
-    hbm = pl.BlockSpec(memory_space=pl.ANY)
+    hbm = pl.BlockSpec(memory_space=pltpu.HBM)
     dma = pltpu.SemaphoreType.DMA
     return pl.pallas_call(
         functools.partial(kernel, seqs, rows, count),
@@ -489,7 +483,7 @@
             pltpu.VMEM((width, 2 * head), BF16),
             pltpu.VMEM((width, head), BF16),
             pltpu.VMEM(gates.shape, BF16),
-            pltpu.VMEM((1, 1), F32),
+            pltpu.SMEM((1,), F32),
             pltpu.VMEM((seqs, 1, rows), F32),
             pltpu.VMEM((1, head), F32),
             pltpu.VMEM((seqs, rows, head), F32),
@@ -512,7 +506,9 @@
             dma((seqs, count)),
             dma((seqs,)),
         ],
-        compiler_params=pltpu.CompilerParams(collective_id=0, has_side_effects=True),
+        compiler_params=pltpu.CompilerParams(
+            collective_id=0, has_side_effects=True, vmem_limit_bytes=GRANT
+        ),
     )(
         tokens,
         decoded_input,
@@ -520,7 +516,7 @@
         key_weight,
         value_weight,
         gates,
-        head_decay_rate.reshape(1, 1),
+        head_decay_rate,
         extra_log_decay,
         read_norm_gain.reshape(1, head),
     )

time: 149 us -> 102 us (0.68)
  Pallas kernels: 145 us -> 98.4 us
    pallas_call x1, Pallas kernels: 145 us -> 98.4 us  [per_device(): pl.pallas_call(functools.partial(kernel, seqs, rows, count), out_shape=(j...]
where the time goes in v4:
time: 102 us
  Pallas kernels  98.4 us (96%)
  local copies, waits for them, and re-layouts  2.4 us (2%)
  between operations  1.29 us (1%)
    pallas_call x1, Pallas kernels, per_device(): pl.pallas_call(functools.partial(kernel, seqs, rows, count), out_shape=(j...  98.4 us
    unnamed x2, local copies, waits for them, and re-layouts  2.4 us

profile of v4, /device:TPU:6, one launch (start us, length us, event | category | flops | bytes accessed | tf_op | source)
XLA Modules:
  0.0 102.1 jit_solution(6364949752588731573)
XLA Ops:
  1.3 98.4 %shard_map.104 = (bf16[2,1,8,128]{3,2,1,0:T(8,128)(2,1)}, bf16[2,128]{1,0:T(2,128)(2,1)}) custom-call(bf16[2,256,2048]{2,1,0:T(8,128)(2,1)} %tok_hbm.1, bf16[2,2048]{1,0:T(2,128)(2,1)} %dec_hbm.1, bf16[2048,128]{1,0:T(8,128)(2,1)} %wq_hbm.1, bf16[2048,128]{1,0:T(8,128)(2,1)} %wk_hbm.1, bf16[2048,128]{1,0:T(8,128)(2,1)} %wv_hbm.1, bf16[64,2048]{1,0:T(8,128)(2,1)} %bitcast.4, ...), custom_call_target="tpu_custom_call" | custom-call | tf_op jit(solution)/shard_map/pallas_call | solution.py:472
  99.7 1.3 %copy.14 = bf16[2,1,8,128]{3,2,1,0:T(8,128)(2,1)} copy(bf16[2,1,8,128]{3,2,1,0:T(8,128)(2,1)} %get-tuple-element.4) | data formatting | bytes 8192
  101.0 1.1 %copy.15 = bf16[2,128]{1,0:T(2,128)(2,1)} copy(bf16[2,128]{1,0:T(2,128)(2,1)} %get-tuple-element.5) | data formatting | bytes 1024

commit v5 on v4

--- a/solution.py
+++ b/solution.py
@@ -13,6 +13,7 @@
 epsilon = 1e-06
 write_offset = 5.0
 BLOCK = 64
+CHUNKS = 4
 GRANT = 60 * 1024 * 1024
 
 
@@ -112,18 +113,21 @@
         copy.start()
         return copy
 
-    load_w = [
-        load(wk_hbm, wkv_ref.at[:, pl.ds(0, head)], 0),
-        load(wv_hbm, wkv_ref.at[:, pl.ds(head, head)], 1),
-    ]
-    load_x = [load(tok_hbm.at[0], x_ref.at[0], 2)]
-    load_g = [
-        load(gate_hbm, gate_ref, 3),
-        load(rate_hbm, rate_ref, 4),
-        load(extra_hbm, extra_ref, 5),
-    ]
-    for s in range(1, seqs):
-        load_x.append(load(tok_hbm.at[s], x_ref.at[s], 8 + s))
+    width = x_ref.shape[-1]
+    wide = width // CHUNKS
+    loads = []
+    for c in range(CHUNKS):
+        cut = pl.ds(c * wide, wide)
+        pairs = [
+            (wk_hbm.at[cut], wkv_ref.at[cut, pl.ds(0, head)]),
+            (wv_hbm.at[cut], wkv_ref.at[cut, pl.ds(head, head)]),
+        ]
+        pairs += [(tok_hbm.at[s, :, cut], x_ref.at[s, :, cut]) for s in range(seqs)]
+        pairs.append((gate_hbm.at[:, cut], gate_ref.at[:, cut]))
+        loads.append(
+            [load(pair[0], pair[1], 8 + c * len(pairs) + i) for i, pair in enumerate(pairs)]
+        )
+    load_g = [load(rate_hbm, rate_ref, 4), load(extra_hbm, extra_ref, 5)]
     load_r = load(gain_hbm, gain_ref, 6)
 
     def at(index):
@@ -146,23 +150,28 @@
     def _():
         greet(last_one)
 
-    for copy in load_w:
+    row_g = iota((gates, rows), 0)
+    sums = [None] * seqs
+    gate_sums = [None] * seqs
+    for c in range(CHUNKS):
+        for copy in loads[c]:
+            copy.wait()
+        cut = slice(c * wide, (c + 1) * wide)
+        for s in range(seqs):
+            part = dot(x_ref[s, :, cut], wkv_ref[cut])
+            sums[s] = part if c == 0 else sums[s] + part
+            part = dot_nt(gate_ref[:, cut], x_ref[s, :, cut])
+            gate_sums[s] = part if c == 0 else gate_sums[s] + part
+    for copy in load_g:
         copy.wait()
-
-    row_g = iota((gates, rows), 0)
     gate_rows = []
     for s in range(seqs):
-        load_x[s].wait()
-        kv = silu(dot(x_ref[s], wkv_ref[...]))
+        kv = silu(sums[s])
         k_ref[s] = unit_rows(kv[:, :head])
         v_ref[s] = kv[:, head:]
-        if s == 0:
-            for copy in load_g:
-                copy.wait()
-        both = dot_nt(gate_ref[...], x_ref[s])
         picked = [
             jnp.sum(jnp.where(row_g == head_index, part, 0.0), axis=0, keepdims=True)
-            for part in (both[:gates], both[gates:])
+            for part in (gate_sums[s][:gates], gate_sums[s][gates:])
         ]
         gate_rows.append(picked)
     rate = rate_ref[0]
@@ -236,36 +245,31 @@
     head_eye = jnp.where(iota((head, head), 0) == iota((head, head), 1), 1.0, 0.0)
     row_b = iota((rows, 1), 0) // BLOCK
     inverse = [diagonal(split(t_mat)) for t_mat in solves]
-    carried, steps = [], []
+    pieces = []
     for s in range(seqs):
         keys = k_ref[s]
-        weights = passes(inverse[s], split(keys * column(2, s)))
+        right = jnp.concatenate([keys * column(2, s), v_ref[s] * column(0, s)], axis=1)
+        solved = passes(inverse[s], split(right))
         kept = keys * column(3, s)
         spans = jnp.concatenate(
             [jnp.where(row_b == b, kept, 0.0) for b in range(blocks)], axis=1
         )
-        carried.append(split(spans))
-        moved = passes(split(jnp.transpose(weights)), carried[s])
-        step = []
+        moved = passes(split(jnp.transpose(solved)), split(spans))
+        piece = []
         for b in range(blocks):
             decay = jnp.exp(total[s : s + 1, b * BLOCK : b * BLOCK + 1])
-            step.append(split(decay * head_eye - moved[:, b * head : (b + 1) * head]))
-        steps.append(step)
-    tails = []
+            part = moved[:, b * head : (b + 1) * head]
+            piece.append((decay * head_eye - part[:head], part[head:]))
+        pieces.append(piece)
+    while len(pieces[0]) > 1:
+        for s in range(seqs):
+            merged = []
+            for early, late in zip(pieces[s][0::2], pieces[s][1::2]):
+                both = product(jnp.concatenate(early, axis=0), late[0])
+                merged.append((both[:head], both[head:] + late[1]))
+            pieces[s] = merged
     for s in range(seqs):
-        step = steps[s]
-        tail = split(passes(step[2], step[3]))
-        tails.append(tail)
-        ab_ref[s, 0] = passes(split(passes(step[0], step[1])), tail)
-
-    def pushes():
-        for s in range(seqs):
-            deltas = passes(inverse[s], split(v_ref[s] * column(0, s)))
-            moved = passes(split(jnp.transpose(deltas)), carried[s])
-            part = [moved[:, b * head : (b + 1) * head] for b in range(blocks)]
-            early = passes(split(part[0]), steps[s][1]) + part[1]
-            late = passes(split(part[2]), steps[s][3]) + part[3]
-            ab_ref[s, 1] = passes(split(early), tails[s]) + late
+        ab_ref[s, 0], ab_ref[s, 1] = pieces[s][0]
 
     def chain(s, half):
         return pltpu.make_async_remote_copy(
@@ -307,32 +311,6 @@
             device_id_type=MESH,
         )
 
-    @pl.when(in_chain)
-    def _():
-        pl.semaphore_wait(barrier, 1)
-
-    for s in range(seqs):
-
-        @pl.when(is_second)
-        def _():
-            tx_ref[s, 0] = ab_ref[s, 0]
-
-        @pl.when(me >= 2)
-        def _():
-            chain(s, 0).wait_recv()
-
-        @pl.when(jnp.logical_and(in_chain, me >= 2))
-        def _():
-            tx_ref[s, 0] = product(rx_ref[s, 0], ab_ref[s, 0])
-
-        @pl.when(in_chain)
-        def _():
-            if s:
-                chain(s - 1, 0).wait_send()
-            chain(s, 0).start()
-
-    pushes()
-
     @pl.when(is_first)
     def _():
         pl.semaphore_wait(barrier, 1)
@@ -340,7 +318,7 @@
             push(s).start()
         copies = [
             pltpu.make_async_copy(dec_hbm, dec_ref, load_sem.at[7]),
-            pltpu.make_async_copy(wq_hbm, wq_ref, load_sem.at[8]),
+            pltpu.make_async_copy(wq_hbm, wq_ref, load_sem.at[3]),
         ]
         for copy in copies:
             copy.start()
@@ -371,38 +349,45 @@
 
     @pl.when(in_chain)
     def _():
-        for s in range(seqs):
-
-            @pl.when(is_second)
-            def _():
-                tx_ref[s, 1] = ab_ref[s, 1]
-
-            @pl.when(jnp.logical_not(is_second))
-            def _():
-                chain(s, 1).wait_recv()
-                tx_ref[s, 1] = product(rx_ref[s, 1], ab_ref[s, 0]) + ab_ref[s, 1]
-
-            if s:
-                chain(s - 1, 1).wait_send()
-            else:
-                chain(seqs - 1, 0).wait_send()
-            chain(s, 1).start()
+        pl.semaphore_wait(barrier, 1)
+        for half in range(2):
+            for s in range(seqs):
+
+                @pl.when(is_second)
+                def _():
+                    tx_ref[s, half] = ab_ref[s, half]
+
+                @pl.when(jnp.logical_not(is_second))
+                def _():
+                    chain(s, half).wait_recv()
+                    moved = product(rx_ref[s, half], ab_ref[s, 0])
+                    tx_ref[s, half] = moved + ab_ref[s, 1] if half else moved
+
+                chain(s, half).start()
 
     @pl.when(is_last)
     def _():
         pl.semaphore_wait(barrier, count - 1)
         load_r.wait()
         decoded.wait_recv()
+        ahead = []
+        for s in range(seqs):
+            step, own = split(ab_ref[s, 0]), ab_ref[s, 1]
+            new = split(new_rx[s])
+            read_step = passes(new, step, dot_nt)
+            ahead.append((step, split(read_step), passes(new, split(own), dot_nt)))
         joins = []
         for s in range(seqs):
+            chain(s, 0).wait_recv()
             push(s).wait_recv()
             joins.append(product(first_ref[s], rx_ref[s, 0]))
         for s in range(seqs):
+            step, read_step, read_own = ahead[s]
             chain(s, 1).wait_recv()
-            joined = joins[s] + rx_ref[s, 1]
-            flipped = product(joined, ab_ref[s, 0]) + ab_ref[s, 1]
+            joined = split(joins[s] + rx_ref[s, 1])
+            flipped = passes(joined, step) + ab_ref[s, 1]
+            reads = passes(read_step, joined, dot_nt) + read_own
             new = new_rx[s]
-            reads = product(new, flipped, dot_nt)
             final = jnp.transpose(flipped)
             key_read, query_read = reads[0:1], reads[1:2]
             value, beta, hold = new[2:3], new[3:4], new[4:5]
@@ -441,7 +426,9 @@
 
     @pl.when(in_chain)
     def _():
-        chain(seqs - 1, 1).wait_send()
+        for half in range(2):
+            for s in range(seqs):
+                chain(s, half).wait_send()
 
     @pl.when(is_last)
     def _():
@@ -496,7 +483,7 @@
             pltpu.VMEM((seqs, 8, head), F32),
             pltpu.VMEM((seqs, count, 2 * each, head), F32),
             pltpu.VMEM((seqs, 2 * each, head), F32),
-            dma((8 + seqs,)),
+            dma((8 + CHUNKS * (seqs + 3),)),
             dma((seqs, 2)),
             dma((seqs, 2)),
             dma((seqs,)),

time: 102 us -> 100 us (0.980)
  Pallas kernels: 98.4 us -> 95.6 us
    pallas_call x1, Pallas kernels: 98.4 us -> 95.6 us  [per_device(): pl.pallas_call(functools.partial(kernel, seqs, rows, count), out_shape=(j...]
where the time goes in v5:
time: 100 us; the launch traced here: 99.3 us
  Pallas kernels  95.6 us (96%)
  local copies, waits for them, and re-layouts  2.4 us (2%)
  between operations  1.29 us (1%)
    pallas_call x1, Pallas kernels, per_device(): pl.pallas_call(functools.partial(kernel, seqs, rows, count), out_shape=(j...  95.6 us
    unnamed x2, local copies, waits for them, and re-layouts  2.4 us

profile of v5, /device:TPU:6, one launch (start us, length us, event | category | flops | bytes accessed | tf_op | source)
XLA Modules:
  0.0 99.3 jit_solution(6142855310996879162)
XLA Ops:
  1.3 95.6 %shard_map.104 = (bf16[2,1,8,128]{3,2,1,0:T(8,128)(2,1)}, bf16[2,128]{1,0:T(2,128)(2,1)}) custom-call(bf16[2,256,2048]{2,1,0:T(8,128)(2,1)} %tok_hbm.1, bf16[2,2048]{1,0:T(2,128)(2,1)} %dec_hbm.1, bf16[2048,128]{1,0:T(8,128)(2,1)} %wq_hbm.1, bf16[2048,128]{1,0:T(8,128)(2,1)} %wk_hbm.1, bf16[2048,128]{1,0:T(8,128)(2,1)} %wv_hbm.1, bf16[64,2048]{1,0:T(8,128)(2,1)} %bitcast.4, ...), custom_call_target="tpu_custom_call" | custom-call | tf_op jit(solution)/shard_map/pallas_call | solution.py:459
  96.9 1.3 %copy.14 = bf16[2,1,8,128]{3,2,1,0:T(8,128)(2,1)} copy(bf16[2,1,8,128]{3,2,1,0:T(8,128)(2,1)} %get-tuple-element.4) | data formatting | bytes 8192
  98.2 1.1 %copy.15 = bf16[2,128]{1,0:T(2,128)(2,1)} copy(bf16[2,128]{1,0:T(2,128)(2,1)} %get-tuple-element.5) | data formatting | bytes 1024

commit v6 on v5

--- a/solution.py
+++ b/solution.py
@@ -14,7 +14,8 @@
 write_offset = 5.0
 BLOCK = 64
 CHUNKS = 4
-GRANT = 60 * 1024 * 1024
+GROUP = 8
+GRANT = 24 << 20
 
 
 def split(x):
@@ -101,10 +102,14 @@
     me = lax.axis_index("sp")
     head_index = lax.axis_index("tp")
     head = k_ref.shape[-1]
-    gates = gate_ref.shape[0] // 2
+    gates = GROUP
+    heads = gate_hbm.shape[0] // 2
+    first = pl.multiple_of(head_index // GROUP * GROUP, GROUP)
+    local_head = lax.rem(head_index, GROUP)
     last_one = count - 1
     is_first = me == 0
     is_second = me == 1
+    is_decoder = me == last_one - 1
     is_last = me == last_one
     in_chain = jnp.logical_and(me > 0, me < last_one)
 
@@ -123,12 +128,25 @@
             (wv_hbm.at[cut], wkv_ref.at[cut, pl.ds(head, head)]),
         ]
         pairs += [(tok_hbm.at[s, :, cut], x_ref.at[s, :, cut]) for s in range(seqs)]
-        pairs.append((gate_hbm.at[:, cut], gate_ref.at[:, cut]))
+        pairs += [
+            (gate_hbm.at[pl.ds(first + g // GROUP * heads, GROUP), cut], gate_ref.at[pl.ds(g, GROUP), cut])
+            for g in (0, GROUP)
+        ]
         loads.append(
             [load(pair[0], pair[1], 8 + c * len(pairs) + i) for i, pair in enumerate(pairs)]
         )
     load_g = [load(rate_hbm, rate_ref, 4), load(extra_hbm, extra_ref, 5)]
     load_r = load(gain_hbm, gain_ref, 6)
+    load_dec = [
+        pltpu.make_async_copy(dec_hbm, dec_ref, load_sem.at[7]),
+        pltpu.make_async_copy(wq_hbm, wq_ref, load_sem.at[3]),
+    ]
+
+    @pl.when(is_decoder)
+    def _():
+        for copy in load_dec:
+            copy.start()
+
 
     def at(index):
         return {"sp": index}
@@ -170,7 +188,7 @@
         k_ref[s] = unit_rows(kv[:, :head])
         v_ref[s] = kv[:, head:]
         picked = [
-            jnp.sum(jnp.where(row_g == head_index, part, 0.0), axis=0, keepdims=True)
+            jnp.sum(jnp.where(row_g == local_head, part, 0.0), axis=0, keepdims=True)
             for part in (gate_sums[s][:gates], gate_sums[s][gates:])
         ]
         gate_rows.append(picked)
@@ -228,10 +246,17 @@
         spread = compact(jnp.broadcast_to(column(1, s), (rows, rows))) - running[s : s + 1]
         below = jnp.where(strict, jnp.exp(jnp.where(strict, spread, 0.0)), 0.0)
         n_mat = compact(jnp.broadcast_to(column(0, s), (rows, rows))) * inner * below
-        pair = row_c // 2 == inside // 2
         n_mats.append(n_mat)
-        solves.append(eye - jnp.where(pair, n_mat, 0.0))
-    depth = 1
+    near = row_c // 8 == inside // 8
+    small = [split(jnp.where(near, n_mat, 0.0)) for n_mat in n_mats]
+    squares = [passes(m, diagonal(m)) for m in small]
+    for s in range(seqs):
+        square = split(squares[s])
+        spread2 = diagonal(square)
+        fourth = passes(square, spread2)
+        start = eye - jnp.where(near, n_mats[s], 0.0) + squares[s] - passes(small[s], spread2)
+        solves.append(start + passes(split(start), diagonal(split(fourth))))
+    depth = 3
     while 1 << depth < BLOCK:
         ri = lax.shift_right_logical(row_c, depth)
         ci = lax.shift_right_logical(inside, depth)
@@ -316,13 +341,28 @@
         pl.semaphore_wait(barrier, 1)
         for s in range(seqs):
             push(s).start()
-        copies = [
-            pltpu.make_async_copy(dec_hbm, dec_ref, load_sem.at[7]),
-            pltpu.make_async_copy(wq_hbm, wq_ref, load_sem.at[3]),
-        ]
-        for copy in copies:
-            copy.start()
-        for copy in copies:
+
+    @pl.when(in_chain)
+    def _():
+        pl.semaphore_wait(barrier, 1)
+        for half in range(2):
+            for s in range(seqs):
+
+                @pl.when(is_second)
+                def _():
+                    tx_ref[s, half] = ab_ref[s, half]
+
+                @pl.when(jnp.logical_not(is_second))
+                def _():
+                    chain(s, half).wait_recv()
+                    moved = product(rx_ref[s, half], ab_ref[s, 0])
+                    tx_ref[s, half] = moved + ab_ref[s, 1] if half else moved
+
+                chain(s, half).start()
+
+    @pl.when(is_decoder)
+    def _():
+        for copy in load_dec:
             copy.wait()
         dec = dec_ref[...]
         new_kv = silu(dot(dec, wkv_ref[...]))
@@ -332,7 +372,7 @@
         both = dot_nt(gate_ref[...], dec)
         row_n = iota((gates, seqs), 0)
         picked = [
-            jnp.sum(jnp.where(row_n == head_index, part, 0.0), axis=0, keepdims=True)
+            jnp.sum(jnp.where(row_n == local_head, part, 0.0), axis=0, keepdims=True)
             for part in (both[:gates], both[gates:])
         ]
         new_beta = jax.nn.sigmoid(picked[0] - write_offset)
@@ -346,24 +386,6 @@
             new_tx[s, 4:5] = jnp.broadcast_to(keep[:, one], (1, head))
             new_tx[s, 5:8] = jnp.zeros((3, head), F32)
         decoded.start()
-
-    @pl.when(in_chain)
-    def _():
-        pl.semaphore_wait(barrier, 1)
-        for half in range(2):
-            for s in range(seqs):
-
-                @pl.when(is_second)
-                def _():
-                    tx_ref[s, half] = ab_ref[s, half]
-
-                @pl.when(jnp.logical_not(is_second))
-                def _():
-                    chain(s, half).wait_recv()
-                    moved = product(rx_ref[s, half], ab_ref[s, 0])
-                    tx_ref[s, half] = moved + ab_ref[s, 1] if half else moved
-
-                chain(s, half).start()
 
     @pl.when(is_last)
     def _():
@@ -422,6 +444,9 @@
     def _():
         for s in range(seqs):
             push(s).wait_send()
+
+    @pl.when(is_decoder)
+    def _():
         decoded.wait_send()
 
     @pl.when(in_chain)
@@ -469,7 +494,7 @@
             pltpu.VMEM((seqs, width), BF16),
             pltpu.VMEM((width, 2 * head), BF16),
             pltpu.VMEM((width, head), BF16),
-            pltpu.VMEM(gates.shape, BF16),
+            pltpu.VMEM((2 * GROUP, width), BF16),
             pltpu.SMEM((1,), F32),
             pltpu.VMEM((seqs, 1, rows), F32),
             pltpu.VMEM((1, head), F32),
@@ -483,7 +508,7 @@
             pltpu.VMEM((seqs, 8, head), F32),
             pltpu.VMEM((seqs, count, 2 * each, head), F32),
             pltpu.VMEM((seqs, 2 * each, head), F32),
-            dma((8 + CHUNKS * (seqs + 3),)),
+            dma((8 + CHUNKS * (seqs + 4),)),
             dma((seqs, 2)),
             dma((seqs, 2)),
             dma((seqs,)),
@@ -496,7 +521,7 @@
         compiler_params=pltpu.CompilerParams(
             collective_id=0, has_side_effects=True, vmem_limit_bytes=GRANT
         ),
-    )(
+    )(*[x if x.shape == (1,) else pltpu.with_memory_space_constraint(x, pltpu.HBM) for x in (
         tokens,
         decoded_input,
         query_weight,
@@ -506,7 +531,7 @@
         head_decay_rate,
         extra_log_decay,
         read_norm_gain.reshape(1, head),
-    )
+    )]    )
 
 
 def solution(mesh):

time: 100 us -> 98.9 us (0.989)
  local copies, waits for them, and re-layouts: 2.4 us -> 1.11 us
    unnamed x2, local copies, waits for them, and re-layouts: 2.4 us -> 1.11 us
where the time goes in v6:
time: 98.9 us; the launch traced here: 98.7 us
  Pallas kernels  96.4 us (97%)
  between operations  1.29 us (1%)
  local copies, waits for them, and re-layouts  1.11 us (1%)
    pallas_call x1, Pallas kernels, per_device(): pl.pallas_call(functools.partial(kernel, seqs, rows, count), out_shape=(j...  96.4 us

profile of v6, /device:TPU:6, one launch (start us, length us, event | category | flops | bytes accessed | tf_op | source)
XLA Modules:
  0.0 98.7 jit_solution(15411145023026817861)
XLA Ops:
  1.3 96.4 %shard_map.104 = (bf16[2,1,8,128]{3,2,1,0:T(8,128)(2,1)S(1)}, bf16[2,128]{1,0:T(2,128)(2,1)S(1)}) custom-call(bf16[2,256,2048]{2,1,0:T(8,128)(2,1)} %tok_hbm.1, bf16[2,2048]{1,0:T(2,128)(2,1)} %dec_hbm.1, bf16[2048,128]{1,0:T(8,128)(2,1)} %wq_hbm.1, bf16[2048,128]{1,0:T(8,128)(2,1)} %wk_hbm.1, bf16[2048,128]{1,0:T(8,128)(2,1)} %wv_hbm.1, ...), custom_call_target="tpu_custom_call" | custom-call | tf_op jit(solution)/shard_map/pallas_call | solution.py:484
  97.6 0.6 copy.14
  98.2 0.5 copy.15

commit v7 on v6

--- a/solution.py
+++ b/solution.py
@@ -33,7 +33,9 @@
 
 
 def passes(a, b, one=dot):
-    return one(a[0], b[0]) + (one(a[0], b[1]) + one(a[1], b[0]))
+    rows = a[0].shape[0]
+    both = one(jnp.concatenate([a[0], a[1]], axis=0), b[0])
+    return both[:rows] + (one(a[0], b[1]) + both[rows:])
 
 
 def product(a, b, one=dot):
@@ -109,7 +111,7 @@
     last_one = count - 1
     is_first = me == 0
     is_second = me == 1
-    is_decoder = me == last_one - 1
+    is_decoder = me == 0
     is_last = me == last_one
     in_chain = jnp.logical_and(me > 0, me < last_one)
 
@@ -239,62 +241,74 @@
     def diagonal(pair):
         return [jnp.concatenate([part * own for own in own_lanes], axis=0) for part in pair]
 
-    n_mats, solves = [], []
-    for s in range(seqs):
-        halves = split(k_ref[s])
+    head_eye = jnp.where(iota((head, head), 0) == iota((head, head), 1), 1.0, 0.0)
+    row_b = iota((rows, 1), 0) // BLOCK
+    near = row_c // 8 == inside // 8
+
+    def solve(s):
+        keys = k_ref[s]
+        halves = split(keys)
         inner = compact(passes(halves, halves, dot_nt))
+        yield
         spread = compact(jnp.broadcast_to(column(1, s), (rows, rows))) - running[s : s + 1]
         below = jnp.where(strict, jnp.exp(jnp.where(strict, spread, 0.0)), 0.0)
+        yield
         n_mat = compact(jnp.broadcast_to(column(0, s), (rows, rows))) * inner * below
-        n_mats.append(n_mat)
-    near = row_c // 8 == inside // 8
-    small = [split(jnp.where(near, n_mat, 0.0)) for n_mat in n_mats]
-    squares = [passes(m, diagonal(m)) for m in small]
-    for s in range(seqs):
-        square = split(squares[s])
-        spread2 = diagonal(square)
-        fourth = passes(square, spread2)
-        start = eye - jnp.where(near, n_mats[s], 0.0) + squares[s] - passes(small[s], spread2)
-        solves.append(start + passes(split(start), diagonal(split(fourth))))
-    depth = 3
-    while 1 << depth < BLOCK:
-        ri = lax.shift_right_logical(row_c, depth)
-        ci = lax.shift_right_logical(inside, depth)
-        mask = jnp.logical_and(ri == ci + 1, lax.bitwise_and(ci, 1) == 0)
-        for s in range(seqs):
-            t_mat = split(solves[s])
-            inner = passes(split(jnp.where(mask, n_mats[s], 0.0)), diagonal(t_mat))
-            solves[s] = solves[s] - passes(t_mat, diagonal(split(inner)))
-        depth += 1
-
-    head_eye = jnp.where(iota((head, head), 0) == iota((head, head), 1), 1.0, 0.0)
-    row_b = iota((rows, 1), 0) // BLOCK
-    inverse = [diagonal(split(t_mat)) for t_mat in solves]
-    pieces = []
-    for s in range(seqs):
-        keys = k_ref[s]
+        small = jnp.where(near, n_mat, 0.0)
+        parts = split(small)
+        square = passes(parts, diagonal(parts))
+        yield
+        halves = split(square)
+        spread2 = diagonal(halves)
+        fourth = passes(halves, spread2)
+        yield
+        start = eye - small + square - passes(parts, spread2)
+        yield
+        solved = start + passes(split(start), diagonal(split(fourth)))
+        yield
+        own = split(solved)
+        spread_own = diagonal(own)
+        lower = jnp.where(near, 0.0, n_mat)
+        first_power = passes(own, diagonal(split(lower)))
+        yield
+        parts = split(first_power)
+        square = passes(parts, diagonal(parts))
+        yield
+        halves = split(square)
+        spread2 = diagonal(halves)
+        fourth = passes(halves, spread2)
+        start = eye - first_power + square - passes(parts, spread2)
+        yield
+        chain8 = start + passes(split(start), diagonal(split(fourth)))
+        yield
+        solved = passes(split(chain8), spread_own)
+        yield
         right = jnp.concatenate([keys * column(2, s), v_ref[s] * column(0, s)], axis=1)
-        solved = passes(inverse[s], split(right))
+        deltas = passes(diagonal(split(solved)), split(right))
+        yield
         kept = keys * column(3, s)
         spans = jnp.concatenate(
             [jnp.where(row_b == b, kept, 0.0) for b in range(blocks)], axis=1
         )
-        moved = passes(split(jnp.transpose(solved)), split(spans))
-        piece = []
+        moved = passes(split(jnp.transpose(deltas)), split(spans))
+        yield
+        pieces = []
         for b in range(blocks):
             decay = jnp.exp(total[s : s + 1, b * BLOCK : b * BLOCK + 1])
             part = moved[:, b * head : (b + 1) * head]
-            piece.append((decay * head_eye - part[:head], part[head:]))
-        pieces.append(piece)
-    while len(pieces[0]) > 1:
-        for s in range(seqs):
+            pieces.append((decay * head_eye - part[:head], part[head:]))
+        while len(pieces) > 1:
             merged = []
-            for early, late in zip(pieces[s][0::2], pieces[s][1::2]):
+            for early, late in zip(pieces[0::2], pieces[1::2]):
                 both = product(jnp.concatenate(early, axis=0), late[0])
                 merged.append((both[:head], both[head:] + late[1]))
-            pieces[s] = merged
-    for s in range(seqs):
-        ab_ref[s, 0], ab_ref[s, 1] = pieces[s][0]
+            pieces = merged
+            yield
+        ab_ref[s, 0], ab_ref[s, 1] = pieces[0]
+        yield
+
+    for _ in zip(*[solve(s) for s in range(seqs)]):
+        pass
 
     def chain(s, half):
         return pltpu.make_async_remote_copy(

time: 98.9 us -> 96.7 us (0.978)
  Pallas kernels: 96.4 us -> 94 us
    pallas_call x1, Pallas kernels: 96.4 us -> 94 us  [per_device(): pl.pallas_call(functools.partial(kernel, seqs, rows, count), out_shape=(j...]
where the time goes in v7:
time: 96.7 us; the launch traced here: 96.4 us
  Pallas kernels  94 us (97%)
  between operations  1.29 us (1%)
  local copies, waits for them, and re-layouts  1.11 us (1%)
    pallas_call x1, Pallas kernels, per_device(): pl.pallas_call(functools.partial(kernel, seqs, rows, count), out_shape=(j...  94 us

profile of v7, /device:TPU:6, one launch (start us, length us, event | category | flops | bytes accessed | tf_op | source)
XLA Modules:
  0.0 96.4 jit_solution(13173003363438494107)
XLA Ops:
  1.3 94.0 %shard_map.104 = (bf16[2,1,8,128]{3,2,1,0:T(8,128)(2,1)S(1)}, bf16[2,128]{1,0:T(2,128)(2,1)S(1)}) custom-call(bf16[2,256,2048]{2,1,0:T(8,128)(2,1)} %tok_hbm.1, bf16[2,2048]{1,0:T(2,128)(2,1)} %dec_hbm.1, bf16[2048,128]{1,0:T(8,128)(2,1)} %wq_hbm.1, bf16[2048,128]{1,0:T(8,128)(2,1)} %wk_hbm.1, bf16[2048,128]{1,0:T(8,128)(2,1)} %wv_hbm.1, ...), custom_call_target="tpu_custom_call" | custom-call | tf_op jit(solution)/shard_map/pallas_call | solution.py:498
  95.2 0.6 copy.14
  95.8 0.5 copy.15

commit v8 on v7

--- a/solution.py
+++ b/solution.py
@@ -33,6 +33,10 @@
 
 
 def passes(a, b, one=dot):
+    if a[0].shape[1] == 128:
+        wide = jnp.concatenate(a, axis=1)
+        twice = jnp.concatenate([b[0], b[0]], axis=0 if one is dot else 1)
+        return one(wide, twice) + one(a[0], b[1])
     rows = a[0].shape[0]
     both = one(jnp.concatenate([a[0], a[1]], axis=0), b[0])
     return both[:rows] + (one(a[0], b[1]) + both[rows:])
@@ -228,7 +232,7 @@
     lane_c = iota((BLOCK, rows), 1)
     inside = lax.bitwise_and(lane_c, BLOCK - 1)
     owner = lane_c // BLOCK
-    own_lanes = [jnp.where(owner == b, 1.0, 0.0).astype(BF16) for b in range(blocks)]
+    own_lanes = [owner == b for b in range(blocks)]
     strict = row_c > inside
     eye = jnp.where(row_c == inside, 1.0, 0.0)
 
@@ -239,7 +243,7 @@
         return out
 
     def diagonal(pair):
-        return [jnp.concatenate([part * own for own in own_lanes], axis=0) for part in pair]
+        return [jnp.concatenate([jnp.where(own, part, jnp.zeros_like(part)) for own in own_lanes], axis=0) for part in pair]
 
     head_eye = jnp.where(iota((head, head), 0) == iota((head, head), 1), 1.0, 0.0)
     row_b = iota((rows, 1), 0) // BLOCK
@@ -270,6 +274,8 @@
         spread_own = diagonal(own)
         lower = jnp.where(near, 0.0, n_mat)
         first_power = passes(own, diagonal(split(lower)))
+        right = jnp.concatenate([keys * column(2, s), v_ref[s] * column(0, s)], axis=1)
+        softened = passes(spread_own, split(right))
         yield
         parts = split(first_power)
         square = passes(parts, diagonal(parts))
@@ -281,17 +287,19 @@
         yield
         chain8 = start + passes(split(start), diagonal(split(fourth)))
         yield
-        solved = passes(split(chain8), spread_own)
-        yield
-        right = jnp.concatenate([keys * column(2, s), v_ref[s] * column(0, s)], axis=1)
-        deltas = passes(diagonal(split(solved)), split(right))
+        deltas = passes(diagonal(split(chain8)), split(softened))
         yield
         kept = keys * column(3, s)
-        spans = jnp.concatenate(
-            [jnp.where(row_b == b, kept, 0.0) for b in range(blocks)], axis=1
-        )
-        moved = passes(split(jnp.transpose(deltas)), split(spans))
-        yield
+        turned = jnp.transpose(deltas)
+        pairs = []
+        for p in range(blocks // 2):
+            cut = slice(2 * p * BLOCK, 2 * (p + 1) * BLOCK)
+            spans = jnp.concatenate(
+                [jnp.where(row_b[cut] == 2 * p + b, kept[cut], 0.0) for b in range(2)], axis=1
+            )
+            pairs.append(product(turned[:, cut], spans))
+        yield
+        moved = jnp.concatenate(pairs, axis=1)
         pieces = []
         for b in range(blocks):
             decay = jnp.exp(total[s : s + 1, b * BLOCK : b * BLOCK + 1])
@@ -405,6 +413,11 @@
     def _():
         pl.semaphore_wait(barrier, count - 1)
         load_r.wait()
+        joins = []
+        for s in range(seqs):
+            chain(s, 0).wait_recv()
+            push(s).wait_recv()
+            joins.append(product(first_ref[s], rx_ref[s, 0]))
         decoded.wait_recv()
         ahead = []
         for s in range(seqs):
@@ -412,11 +425,6 @@
             new = split(new_rx[s])
             read_step = passes(new, step, dot_nt)
             ahead.append((step, split(read_step), passes(new, split(own), dot_nt)))
-        joins = []
-        for s in range(seqs):
-            chain(s, 0).wait_recv()
-            push(s).wait_recv()
-            joins.append(product(first_ref[s], rx_ref[s, 0]))
         for s in range(seqs):
             step, read_step, read_own = ahead[s]
             chain(s, 1).wait_recv()

time: 96.7 us -> 96.2 us (level)
  no operation moved by 1% of the time
where the time goes in v8:
time: 96.2 us; the launch traced here: 96.1 us
  Pallas kernels  93.7 us (97%)
  between operations  1.29 us (1%)
  local copies, waits for them, and re-layouts  1.11 us (1%)
    pallas_call x1, Pallas kernels, per_device(): pl.pallas_call(functools.partial(kernel, seqs, rows, count), out_shape=(j...  93.7 us

profile of v8, /device:TPU:6, one launch (start us, length us, event | category | flops | bytes accessed | tf_op | source)
XLA Modules:
  0.0 96.1 jit_solution(8475702054945196574)
XLA Ops:
  1.3 93.7 %shard_map.104 = (bf16[2,1,8,128]{3,2,1,0:T(8,128)(2,1)S(1)}, bf16[2,128]{1,0:T(2,128)(2,1)S(1)}) custom-call(bf16[2,256,2048]{2,1,0:T(8,128)(2,1)} %tok_hbm.1, bf16[2,2048]{1,0:T(2,128)(2,1)} %dec_hbm.1, bf16[2048,128]{1,0:T(8,128)(2,1)} %wq_hbm.1, bf16[2048,128]{1,0:T(8,128)(2,1)} %wk_hbm.1, bf16[2048,128]{1,0:T(8,128)(2,1)} %wv_hbm.1, ...), custom_call_target="tpu_custom_call" | custom-call | tf_op jit(solution)/shard_map/pallas_call | solution.py:506
  95.0 0.6 copy.14
  95.6 0.5 copy.15

commit v9 on v8

--- a/solution.py
+++ b/solution.py
@@ -14,6 +14,7 @@
 write_offset = 5.0
 BLOCK = 64
 CHUNKS = 4
+NEAR = 3
 GROUP = 8
 GRANT = 24 << 20
 
@@ -444,9 +445,12 @@
             each = head // count
             out_tx[s, :, :each] = cache.reshape(count, each, head)
             out_tx[s, :, each:] = jnp.broadcast_to(read.reshape(1, 1, head), (count, each, head))
-            for k in range(1, count):
+            for k in range(1, NEAR):
                 rows_to(s, k).start()
             out_rx[s] = out_tx[s, last_one]
+        for s in range(seqs):
+            for k in range(NEAR, count):
+                rows_to(s, k).start()
 
     for s in range(seqs):
 

time: 96.2 us -> 96.2 us (level)
  no operation moved by 1% of the time
where the time goes in v9:
time: 96.2 us; the launch traced here: 96.1 us
  Pallas kernels  93.7 us (97%)
  between operations  1.29 us (1%)
  local copies, waits for them, and re-layouts  1.11 us (1%)
    pallas_call x1, Pallas kernels, per_device(): pl.pallas_call(functools.partial(kernel, seqs, rows, count), out_shape=(j...  93.7 us

profile of v9, /device:TPU:6, one launch (start us, length us, event | category | flops | bytes accessed | tf_op | source)
XLA Modules:
  0.0 96.1 jit_solution(2815346666894807604)
XLA Ops:
  1.3 93.7 %shard_map.104 = (bf16[2,1,8,128]{3,2,1,0:T(8,128)(2,1)S(1)}, bf16[2,128]{1,0:T(2,128)(2,1)S(1)}) custom-call(bf16[2,256,2048]{2,1,0:T(8,128)(2,1)} %tok_hbm.1, bf16[2,2048]{1,0:T(2,128)(2,1)} %dec_hbm.1, bf16[2048,128]{1,0:T(8,128)(2,1)} %wq_hbm.1, bf16[2048,128]{1,0:T(8,128)(2,1)} %wk_hbm.1, bf16[2048,128]{1,0:T(8,128)(2,1)} %wv_hbm.1, ...), custom_call_target="tpu_custom_call" | custom-call | tf_op jit(solution)/shard_map/pallas_call | solution.py:510
  95.0 0.6 copy.14
  95.6 0.5 copy.15

commit v10 on v9

--- a/solution.py
+++ b/solution.py
@@ -116,6 +116,7 @@
     last_one = count - 1
     is_first = me == 0
     is_second = me == 1
+    goes_first = lax.rem(head_index, 2) == 0
     is_decoder = me == 0
     is_last = me == last_one
     in_chain = jnp.logical_and(me > 0, me < last_one)
@@ -381,7 +382,14 @@
                     moved = product(rx_ref[s, half], ab_ref[s, 0])
                     tx_ref[s, half] = moved + ab_ref[s, 1] if half else moved
 
-                chain(s, half).start()
+                @pl.when(goes_first)
+                def _():
+                    chain(s, half).start()
+
+            @pl.when(jnp.logical_not(goes_first))
+            def _():
+                for s in range(seqs):
+                    chain(s, half).start()
 
     @pl.when(is_decoder)
     def _():

time: 96.2 us -> 97.1 us (level)
  no operation moved by 1% of the time
where the time goes in v10:
time: 97.1 us; the launch traced here: 96.9 us
  Pallas kernels  94.5 us (97%)
  between operations  1.29 us (1%)
  local copies, waits for them, and re-layouts  1.11 us (1%)
    pallas_call x1, Pallas kernels, per_device(): pl.pallas_call(functools.partial(kernel, seqs, rows, count), out_shape=(j...  94.5 us

profile of v10, /device:TPU:6, one launch (start us, length us, event | category | flops | bytes accessed | tf_op | source)
XLA Modules:
  0.0 96.9 jit_solution(8029978033233642945)
XLA Ops:
  1.3 94.5 %shard_map.104 = (bf16[2,1,8,128]{3,2,1,0:T(8,128)(2,1)S(1)}, bf16[2,128]{1,0:T(2,128)(2,1)S(1)}) custom-call(bf16[2,256,2048]{2,1,0:T(8,128)(2,1)} %tok_hbm.1, bf16[2,2048]{1,0:T(2,128)(2,1)} %dec_hbm.1, bf16[2048,128]{1,0:T(8,128)(2,1)} %wq_hbm.1, bf16[2048,128]{1,0:T(8,128)(2,1)} %wk_hbm.1, bf16[2048,128]{1,0:T(8,128)(2,1)} %wv_hbm.1, ...), custom_call_target="tpu_custom_call" | custom-call | tf_op jit(solution)/shard_map/pallas_call | solution.py:518
  95.8 0.6 copy.14
  96.4 0.5 copy.15
